TPU v7x, 512 devices: a whole 4x8x8 slice. The times are simulated.
512 devices in a mesh: sp: 64 (over z, y), fs: 4 (over x), tp: 2 (over core).
Axes of the slice: x: 4, y: 8, z: 8, core: 2. Of those that a mesh axis runs over, the one named last changes fastest.
Arguments:
- tokens: bfloat16 [4, 8192, 2048], P('fs', ('sp', 'tp')), may hold values from -6 to 6
- norm_gain: float32 [2048], replicated, may hold values from 0.1 to 1.9
- gla_query_weight: bfloat16 [2048, 512], P('sp', 'tp'), may hold values from -0.125 to 0.125
- gla_key_weight: bfloat16 [2048, 512], P('sp', 'tp'), may hold values from -0.125 to 0.125
- gla_value_weight: bfloat16 [2048, 1024], P('sp', 'tp'), may hold values from -0.125 to 0.125
- decay_down: bfloat16 [2048, 32], P('sp'), may hold values from -0.125 to 0.125
- decay_up: bfloat16 [32, 512], P(None, 'tp'), may hold values from -1 to 1
- decay_bias: float32 [512], P('tp'), may hold values from 0.5 to 12
- head_gain: float32 [128], replicated, may hold values from 0.1 to 1.9
- window_query_weight: bfloat16 [2048, 1024], P('sp', 'tp'), may hold values from -3 to 3
- window_key_weight: bfloat16 [2048, 256], P('sp', 'tp'), may hold values from -3 to 3
- window_value_weight: bfloat16 [2048, 256], P('sp', 'tp'), may hold values from -0.125 to 0.125
- sink_logit: float32 [16], P('tp'), may hold values from 3 to 7
- gla_output_weight: bfloat16 [1024, 2048], P('tp', 'sp'), may hold values from -0.125 to 0.125
- window_output_weight: bfloat16 [1024, 2048], P('tp', 'sp'), may hold values from -0.125 to 0.125
Outputs:
- mixed: bfloat16 [4, 8192, 2048], P('fs', ('sp', 'tp'))
All inputs are finite; a program needn't handle non-finite values.
Results may differ from a plain program's by a relative error of at most 0.013.
Values may be sent and summed in bfloat16 or wider, within the bound.
A program may use at most 64 MiB of HBM per device.

v0:
```python
import jax
import jax.numpy as jnp
from jax import lax
from jax.sharding import Mesh
from jax.sharding import PartitionSpec as P

KEY_DIM = 64
VALUE_DIM = 128
SWA_HEADS = 16
KV_HEADS = 4
HEAD_DIM = 64
WINDOW = 128
SPAN = 64
SP = ("sp_0", "sp_1")
SP_TP = ("sp_0", "sp_1", "tp")


EPS = 1e-06
SOFTMAX_TEMPER = 16.0
HIGH = lax.Precision.HIGHEST


def sent_to_all(value, axis):
    peers = lax.axis_size(axis)
    return lax.all_to_all(
        jnp.broadcast_to(value[None], (peers, *value.shape)), axis, 0, 0, tiled=True
    )


def laid_out(blocks, dim):
    dims = list(blocks.shape[1:])
    dims[dim] *= blocks.shape[0]
    return jnp.moveaxis(blocks, 0, dim).reshape(dims)


def gather_directly(value, axis, dim):
    blocks = sent_to_all(value, axis)
    return laid_out(blocks, dim)


def side_by_side(arrays, axis, dim, along):
    both = jnp.concatenate(arrays, axis=along)
    result, at, finished = (lax.all_gather(both, axis, axis=dim, tiled=True), 0, [])
    for a in arrays:
        finished.append(lax.slice_in_dim(result, at, at + a.shape[along], axis=along))
        at += a.shape[along]
    return tuple(finished)


def gather_turned(arrays, axis, dims):
    turned = [jnp.moveaxis(a, dim, 0) for a, dim in zip(arrays, dims)]
    both = jnp.concatenate([t.reshape(len(t), -1) for t in turned], axis=1)
    result, at, finished = (lax.all_gather(both, axis, axis=0, tiled=True), 0, [])
    for t, dim in zip(turned, dims):
        slab = result[:, at : at + t[0].size].reshape(-1, *t.shape[1:])
        finished.append(jnp.moveaxis(slab, 0, dim))
        at += t[0].size
    return tuple(finished)


def nothing_yet(value, identity):
    return jax.tree.map(
        lambda a, e: jnp.broadcast_to(jnp.asarray(e, a.dtype), a.shape), value, identity
    )


def carried_in(value, axes, combine, identity):
    before = start = nothing_yet(value, identity)
    subtotal = value
    for axis in reversed(axes):
        peers, place = (lax.axis_size(axis), lax.axis_index(axis))
        pieces = jax.tree.map(lambda part: lax.all_gather(part, axis), subtotal)
        inside, subtotal = (start, start)
        for k in range(peers):
            passed = k < place
            subtotal = combine(subtotal, jax.tree.map(lambda part: part[k], pieces))
            inside = jax.tree.map(lambda new, old: jnp.where(passed, new, old), subtotal, inside)
        before = combine(inside, before)
    return before


def passed_along(value, axis, by):
    peers = lax.axis_size(axis)
    pairs = [(i, i + by) for i in range(peers) if 0 <= i + by < peers]
    return lax.ppermute(value, axis, pairs)


def split_up(value, dim, peers):
    dims = value.shape
    blocks = value.reshape(*dims[:dim], peers, dims[dim] // peers, *dims[dim + 1 :])
    return jnp.moveaxis(blocks, dim, 0)


def summed_on_arrival(value, axis, dim):
    blocks = split_up(value, dim, lax.axis_size(axis))
    arrived = lax.all_to_all(blocks, axis, split_axis=0, concat_axis=0, tiled=True)
    return arrived.astype(jnp.float32).sum(axis=0)


def rms_rows(values, gain):
    mean_square = jnp.mean(values * values, axis=-1, keepdims=True)
    return values * lax.rsqrt(mean_square + EPS) * gain


def block_terms(query_rows, key_rows, value_rows, log_decay_rate, block_len):
    seq_len, head_count, key_width = query_rows.shape
    value_width = value_rows.shape[-1]
    block_count = seq_len // block_len
    q_scaled = query_rows.reshape(block_count, block_len, head_count, key_width) * key_width ** (
        -0.5
    )
    k_blocks = key_rows.reshape(block_count, block_len, head_count, key_width)
    v_blocks = value_rows.reshape(block_count, block_len, head_count, value_width)
    within = jnp.cumsum(
        log_decay_rate.reshape(block_count, block_len, head_count, key_width), axis=1
    )
    block_total = within[:, -1]
    q_dec = q_scaled * jnp.exp(within)
    k_dec = k_blocks * jnp.exp(-within)
    k_end = k_blocks * jnp.exp(block_total[:, None] - within)
    causal = jnp.tril(jnp.ones((block_len, block_len), dtype=bool))
    scores = jnp.einsum("nihd,njhd->nhij", q_dec, k_dec, precision=HIGH)
    scores = jnp.where(causal, scores, 0.0)
    local_out = jnp.einsum("nhij,njhe->nihe", scores, v_blocks, precision=HIGH)
    update = jnp.einsum("njhd,njhe->nhde", k_end, v_blocks, precision=HIGH)

    def advance(carried, inputs):
        update_in, decay_in = inputs
        return (decay_in[..., None] * carried + update_in, carried)

    start_state = jnp.zeros((head_count, key_width, value_width), jnp.float32)
    last_state, entering = lax.scan(advance, start_state, (update, jnp.exp(block_total)))
    return (q_dec, local_out, entering, last_state, block_total)


def window_band_mask(block_count, block_len, offset):
    query_pos = jnp.arange(block_len)[:, None] + block_len
    key_pos = jnp.arange(2 * block_len)[None, :]
    distance = query_pos - key_pos
    inside = (distance >= 0) & (distance < block_len)
    global_key = (
        offset + jnp.arange(block_count)[:, None, None] * block_len - block_len + key_pos[None]
    )
    return inside[None] & (global_key >= 0)


def window_attend(query_blocks, key_band, value_band, valid, sinks):
    scores = jnp.einsum(
        "nqhgd,nkhd->nhgqk", query_blocks, key_band, preferred_element_type=jnp.float32
    )
    scores = scores * HEAD_DIM ** (-0.5)
    scores = jnp.where(valid[:, None, None], scores, -1e30)
    sink_term = sinks[None, :, :, None, None]
    top = jnp.maximum(jnp.max(scores, axis=-1, keepdims=True), sink_term)
    expo = jnp.exp(scores - top)
    denom = jnp.sum(expo, axis=-1, keepdims=True) + jnp.exp(sink_term - top)
    weights = (expo / denom).astype(jnp.bfloat16)
    attended = jnp.einsum(
        "nhgqk,nkhd->nqhgd", weights, value_band, preferred_element_type=jnp.float32
    )
    return attended.astype(jnp.bfloat16)


def per_device(
    tokens,
    norm_gain,
    gla_query_weight,
    gla_key_weight,
    gla_value_weight,
    decay_down,
    decay_up,
    decay_bias,
    head_gain,
    window_query_weight,
    window_key_weight,
    window_value_weight,
    sink_logit,
    gla_output_weight,
    window_output_weight,
):
    seq_rows = gather_directly(tokens, "tp", 1)[0]
    tok_rows = seq_rows.shape[0]
    input_maps = side_by_side(
        (
            gla_query_weight,
            gla_key_weight,
            gla_value_weight,
            decay_down,
            window_query_weight,
            window_key_weight,
            window_value_weight,
        ),
        SP,
        0,
        1,
    )
    output_maps = gather_turned((gla_output_weight, window_output_weight), SP, (1, 1))
    normed = rms_rows(seq_rows.astype(jnp.float32), norm_gain).astype(jnp.bfloat16)

    def project(weight):
        return jnp.dot(normed, weight, preferred_element_type=jnp.float32).astype(jnp.bfloat16)

    seq_offset = lax.axis_index(SP) * tok_rows
    window_query = project(input_maps[4])
    sliding_key = project(input_maps[5])
    window_value = project(input_maps[6])
    kv_local = sliding_key.shape[1] // HEAD_DIM
    group_size = SWA_HEADS // KV_HEADS
    block_count = tok_rows // WINDOW
    edge_keys, edge_values = passed_along((sliding_key, window_value), SP, 1)

    def banded(rows, edge_rows):
        blocks = rows.reshape(block_count, WINDOW, kv_local, HEAD_DIM)
        edge_block = edge_rows.reshape(1, WINDOW, kv_local, HEAD_DIM)
        earlier = jnp.concatenate([edge_block, blocks[:-1]], axis=0)
        return jnp.concatenate([earlier, blocks], axis=1)

    query_blocks = window_query.reshape(block_count, WINDOW, kv_local, group_size, HEAD_DIM)
    valid = window_band_mask(block_count, WINDOW, seq_offset)
    sinks = sink_logit.reshape(kv_local, group_size)
    attended = window_attend(
        query_blocks,
        banded(sliding_key, edge_keys),
        banded(window_value, edge_values),
        valid,
        sinks,
    )
    window_hidden = attended.reshape(tok_rows, kv_local * group_size * HEAD_DIM)
    gla_query = project(input_maps[0])
    gla_key = project(input_maps[1])
    gla_value = project(input_maps[2])
    low_rank = project(input_maps[3])
    gate_logit_values = jnp.dot(low_rank, decay_up, preferred_element_type=jnp.float32) + decay_bias
    log_decay_rate = jax.nn.log_sigmoid(gate_logit_values) / SOFTMAX_TEMPER
    local_heads = gla_query.shape[1] // KEY_DIM
    q_dec, local_out, entering, last_state, block_total = block_terms(
        gla_query.astype(jnp.float32).reshape(tok_rows, local_heads, KEY_DIM),
        gla_key.astype(jnp.float32).reshape(tok_rows, local_heads, KEY_DIM),
        gla_value.astype(jnp.float32).reshape(tok_rows, local_heads, VALUE_DIM),
        log_decay_rate.reshape(tok_rows, local_heads, KEY_DIM),
        SPAN,
    )
    device_decay = jnp.exp(jnp.sum(block_total, axis=0))

    def combine(earlier, later):
        return (later[1][..., None] * earlier[0] + later[0], earlier[1] * later[1])

    identity = (jnp.zeros_like(last_state), jnp.ones_like(device_decay))
    incoming = carried_in((last_state, device_decay), SP, combine, identity)[0]
    before = jnp.cumsum(block_total, axis=0) - block_total
    entering_all = entering + jnp.exp(before)[..., None] * incoming[None]
    gla_out = local_out + jnp.einsum("nihd,nhde->nihe", q_dec, entering_all, precision=HIGH)
    gla_out = gla_out.reshape(tok_rows, local_heads, VALUE_DIM)
    gla_hidden = (
        rms_rows(gla_out, head_gain).astype(jnp.bfloat16).reshape(tok_rows, local_heads * VALUE_DIM)
    )
    own_rows = tok_rows // lax.axis_size("tp")
    total = jnp.dot(gla_hidden, output_maps[0], preferred_element_type=jnp.float32)
    mixed = summed_on_arrival(
        (total + jnp.dot(window_hidden, output_maps[1], preferred_element_type=jnp.float32)).astype(
            jnp.bfloat16
        ),
        "tp",
        0,
    )
    return mixed.astype(jnp.bfloat16).reshape(1, own_rows, mixed.shape[1])


def solution(mesh):
    split = Mesh(
        mesh.devices.reshape(8, 8, mesh.shape["fs"], mesh.shape["tp"]), ("sp_0", "sp_1", "fs", "tp")
    )
    return jax.shard_map(
        per_device,
        mesh=split,
        in_specs=(
            P("fs", SP_TP, None),
            P(),
            P(SP, "tp"),
            P(SP, "tp"),
            P(SP, "tp"),
            P(SP, None),
            P(None, "tp"),
            P("tp"),
            P(),
            P(SP, "tp"),
            P(SP, "tp"),
            P(SP, "tp"),
            P("tp"),
            P("tp", SP),
            P("tp", SP),
        ),
        out_specs=P("fs", SP_TP, None),
        check_vma=False,
    )
```

profile of v0, /device:TPU:1, one launch (start us, length us, event | category | flops | bytes accessed | tf_op | source)
XLA Modules:
  0.0 308.5 jit_solution(5424452987641162957)
XLA Ops:
  6.5 1.6 concatenate.12
  8.2 1.8 broadcast_in_dim.36
  10.0 10.3 %all-to-all-start = ((bf16[2,1,64,2048]{3,2,1,0:T(8,128)(2,1)}), bf16[2,1,64,2048]{3,2,1,0:T(8,128)(2,1)S(1)}, u32[]{:S(2)}, u32[]{:S(2)}) async-start(bf16[2,1,64,2048]{3,2,1,0:T(8,128)(2,1)} %broadcast_in_dim.36), calls=%async_computation | async-start | bytes 1048576 | tf_op jit(solution)/shard_map/all_to_all | solution.py:25
  20.3 1.4 all-to-all-done
  21.7 0.2 multiply_reduce_fusion
  22.0 0.9 fusion.25
  22.9 89.3 %all-gather.8.cloned.1.call-done = bf16[2048,1824]{1,0:T(8,128)(2,1)} async-done(((bf16[32,1824]{1,0:T(8,128)(2,1)}), bf16[2048,1824]{1,0:T(8,128)(2,1)}) %all-gather.8.cloned.1.call-update) | async-done | bytes 7471120 | tf_op jit(solution)/shard_map/all_gather | solution.py:43
  112.2 1.6 fusion.43
  113.8 0.2 reshape_reshape.14
  114.2 1.5 fusion.20
  115.7 0.2 mul.363
  115.9 1.5 fusion.18
  117.4 0.2 reshape.294
  117.6 2.0 fusion.11
  119.7 0.2 exponential_multiply_fusion
  119.9 0.4 fusion.34
  120.3 0.4 while.13
  120.3 0.1 bitcast_add_fusion.2
  120.5 0.1 bitcast_add_fusion.2
  120.7 0.6 copy-done.1
  121.4 18.4 %all-gather.2 = f32[8,4,64]{2,1,0:T(4,128)S(1)} all-gather(f32[1,4,64]{2,1,0:T(4,128)S(1)} %exponential_bitcast_fusion), channel_id=2, replica_groups=mesh['sp_0'=8,'sp_1'=8,'fs'=4,'tp'=2] {'sp_1'}, dimensions={0}, use_global_device_ids=true | all-gather | bytes 9216 | tf_op jit(solution)/shard_map/all_gather | solution.py:72
  139.8 15.8 %all-gather.14.cloned.1.call-done = f32[32,64,128]{2,1,0:T(8,128)} async-done(((f32[4,64,128]{2,1,0:T(8,128)}), f32[32,64,128]{2,1,0:T(8,128)}) %all-gather.14.cloned.1.call-update) | async-done | bytes 1048592 | tf_op jit(solution)/shard_map/all_gather | solution.py:72
  155.7 2.4 fusion.48
  158.1 0.6 pad_maximum_fusion
  159.1 1.9 convolution_convert_fusion.3
  160.9 2.7 collective-permute-start.1
  163.7 19.2 %all_gather.26 = f32[8,4,64]{2,1,0:T(4,128)S(1)} all-gather(f32[1,4,64]{2,1,0:T(4,128)S(1)} %get-tuple-element.80), channel_id=1, replica_groups=mesh['sp_0'=8,'sp_1'=8,'fs'=4,'tp'=2] {'sp_0'}, dimensions={0}, use_global_device_ids=true | all-gather | bytes 9216 | tf_op jit(solution)/shard_map/all_gather | solution.py:72
  182.9 0.5 convolution_select_fusion
  183.5 0.3 fusion.66
  183.7 1.9 convolution_convert_fusion.4
  185.6 2.6 fusion.14
  188.3 0.1 copy.58
  188.4 2.4 collective-permute-start
  190.8 0.4 fusion.81
  191.2 0.2 fusion.26
  191.4 0.3 collective-permute-done
  191.8 0.3 convolution_convert_fusion
  192.1 7.2 %all-gather.10.cloned.1.call-done = f32[8,4,64,128]{3,2,1,0:T(8,128)} async-done(((f32[1,4,64,128]{3,2,1,0:T(8,128)}), f32[8,4,64,128]{3,2,1,0:T(8,128)}) %all-gather.10.cloned.1.call-update) | async-done | bytes 1048592 | tf_op jit(solution)/shard_map/all_gather | solution.py:72
  199.3 1.9 fusion.47
  201.2 0.6 multiply_reduce_fusion.1
  201.8 0.1 copy.63
  201.9 0.2 copy.55
  202.1 85.4 %all-gather.12.cloned.1.call-done = bf16[2048,1024]{1,0:T(8,128)(2,1)} async-done(((bf16[32,1024]{1,0:T(8,128)(2,1)}), bf16[2048,1024]{1,0:T(8,128)(2,1)}) %all-gather.12.cloned.1.call-update) | async-done | bytes 4194320 | tf_op jit(solution)/shard_map/all_gather | solution.py:53
  287.5 0.2 mul.428
  287.7 2.4 fusion.4
  290.1 2.4 fusion
  292.6 8.6 %all_to_all.10 = bf16[2,64,2048]{2,1,0:T(8,128)(2,1)S(1)} all-to-all(bf16[2,64,2048]{2,1,0:T(8,128)(2,1)S(1)} %bitcast.233), channel_id=1, replica_groups=mesh['sp_0'=8,'sp_1'=8,'fs'=4,'tp'=2] {'tp'}, dimensions={0} | all-to-all | bytes 1048576 | tf_op jit(solution)/shard_map/all_to_all | solution.py:96
  301.1 0.8 reduce_sum.52
  (50 shorter events, 0.9 us)
Async XLA Ops:
  6.5 105.7 %copy-start = (bf16[32,256]{1,0:T(8,128)(2,1)S(1)}, bf16[32,256]{1,0:T(8,128)(2,1)}, u32[]{:S(2)}) copy-start(bf16[32,256]{1,0:T(8,128)(2,1)} %param.23) | copy-start | bytes 49156
  6.5 105.7 %all-gather.8.cloned.1.call-start = ((), (), s32[]{:S(2)}) async-start(), calls=%async_computation.2 | async-start | bytes 7987200 | tf_op jit(solution)/shard_map/all_gather | solution.py:43
  10.0 11.7 %all-to-all-start = ((bf16[2,1,64,2048]{3,2,1,0:T(8,128)(2,1)}), bf16[2,1,64,2048]{3,2,1,0:T(8,128)(2,1)S(1)}, u32[]{:S(2)}, u32[]{:S(2)}) async-start(bf16[2,1,64,2048]{3,2,1,0:T(8,128)(2,1)} %broadcast_in_dim.36), calls=%async_computation | async-start | bytes 1048576 | tf_op jit(solution)/shard_map/all_to_all | solution.py:25
  20.3 135.4 %all-gather.14.cloned.1.call-start = ((), (), s32[]{:S(2)}) async-start(), calls=%async_computation.5 | async-start | bytes 1179648 | tf_op jit(solution)/shard_map/all_gather | solution.py:72
  114.1 44.0 %copy-start.4 = (bf16[512,32]{0,1:T(8,128)(2,1)S(1)}, bf16[512,32]{0,1:T(8,128)(2,1)}, u32[]{:S(2)}) copy-start(bf16[512,32]{0,1:T(8,128)(2,1)} %param.31) | copy-start | bytes 98308
  114.1 44.0 %copy-start.5 = (bf16[512,32]{0,1:T(8,128)(2,1)S(1)}, bf16[512,32]{0,1:T(8,128)(2,1)}, u32[]{:S(2)}) copy-start(bf16[512,32]{0,1:T(8,128)(2,1)} %param.30) | copy-start | bytes 98308
  114.1 44.7 %copy-start.7 = (f32[8]{0:T(128)S(1)}, f32[8]{0:T(128)}, u32[]{:S(2)}) copy-start(f32[8]{0:T(128)} %param.29) | copy-start | bytes 100
  114.2 44.8 %copy-start.6 = (f32[128]{0:T(128)S(1)}, f32[128]{0:T(128)}, u32[]{:S(2)}) copy-start(f32[128]{0:T(128)} %param.25) | copy-start | bytes 1540
  120.6 0.7 copy-start.1
  121.3 78.0 %all-gather.10.cloned.1.call-start = ((), (), s32[]{:S(2)}) async-start(), calls=%async_computation.3 | async-start | bytes 1179648 | tf_op jit(solution)/shard_map/all_gather | solution.py:72
  155.7 43.6 %copy-start.2 = (f32[32,64,128]{2,1,0:T(8,128)S(1)}, f32[32,64,128]{2,1,0:T(8,128)}, u32[]{:S(2)}) copy-start(f32[32,64,128]{2,1,0:T(8,128)} %all-gather.14.cloned.1.call-done) | copy-start | bytes 3145732
  158.0 41.3 %copy-start.3 = (f32[1,4,64,128]{3,2,1,0:T(8,128)S(1)}, f32[1,4,64,128]{3,2,1,0:T(8,128)}, u32[]{:S(2)}) copy-start(f32[1,4,64,128]{3,2,1,0:T(8,128)} %get-tuple-element.63) | copy-start | bytes 393220
  158.1 129.4 %all-gather.12.cloned.1.call-start = ((), (), s32[]{:S(2)}) async-start(), calls=%async_computation.4 | async-start | bytes 4259840 | tf_op jit(solution)/shard_map/all_gather | solution.py:53
  160.9 29.8 %collective-permute-start.1 = (bf16[128,128]{0,1:T(8,128)(2,1)S(1)}, bf16[128,128]{0,1:T(8,128)(2,1)S(1)}, u32[]{:S(2)}, u32[]{:S(2)}) collective-permute-start(bf16[128,128]{0,1:T(8,128)(2,1)S(1)} %convolution_convert_fusion.3), channel_id=1, source_target_pairs={{0,8},{8,16},{16,24},{24,32},{32,40},{40,48},{48,56},{56,64},{64,7... | collective-permute-start | bytes 98312 | tf_op jit(solution)/shard_map/ppermute | solution.py:85
  188.4 3.4 %collective-permute-start = (bf16[128,128]{0,1:T(8,128)(2,1)S(1)}, bf16[128,128]{0,1:T(8,128)(2,1)S(1)}, u32[]{:S(2)}, u32[]{:S(2)}) collective-permute-start(bf16[128,128]{0,1:T(8,128)(2,1)S(1)} %convolution_convert_fusion.4), channel_id=1, source_target_pairs={{0,8},{8,16},{16,24},{24,32},{32,40},{40,48},{48,56},{56,64},{64,7... | collective-permute-start | bytes 98312 | tf_op jit(solution)/shard_map/ppermute | solution.py:85
Sparse Core Ops, SparseCore 0:
  10.3 101.8 all-gather.7
  121.4 34.1 all-gather.13
  158.2 41.0 all-gather.9
  202.2 85.2 all-gather.11
where the time goes:
time: 309 us
  waiting for transfers between devices  200 us (65%)
  blocking collectives  46.2 us (15%)
  matrix products  20.4 us (7%)
  starting transfers between devices  15.5 us (5%)
  between operations  13.5 us (4%)
  other arithmetic  7.83 us (3%)
  local copies, waits for them, and re-layouts  5.43 us (2%)
    all_gather x1, waiting for transfers between devices, side_by_side(): lax.all_gather(both, axis, axis=dim, tiled=True)  89.3 us
    all_gather x1, waiting for transfers between devices, gather_turned(): lax.all_gather(both, axis, axis=0, tiled=True)  85.4 us
    all_gather x2, blocking collectives, carried_in(): pieces = jax.tree.map(lambda part: lax.all_gather(part, axis), subtotal)  37.6 us
    all_gather x2, waiting for transfers between devices, carried_in(): pieces = jax.tree.map(lambda part: lax.all_gather(part, axis), subtotal)  23.1 us
    dot_general x6, matrix products, project(): jnp.dot(normed, weight, preferred_element_type=jnp.float32)  11.5 us
    all_to_all x1, starting transfers between devices, sent_to_all(): lax.all_to_all(jnp.broadcast_to(value[None], (peers, *value.shape)), axis...  10.3 us
    all_to_all x1, blocking collectives, summed_on_arrival(): lax.all_to_all(blocks, axis, split_axis=0, concat_axis=0, tiled=True)  8.59 us
  transfers between devices with their start and end apart: 7, of which 6 were waited for; matrix products, arithmetic and copies ran while one was open for 5% of the time, Pallas kernels for 0%

commit v1 on v0

v1 whole, which is shorter than its diff:
```python
import jax
import jax.numpy as jnp
from jax import lax
from jax.sharding import Mesh
from jax.sharding import PartitionSpec as P

KEY_DIM = 64
VALUE_DIM = 128
HEAD_DIM = 64
WINDOW = 128
SPAN = 64
SP = ("sp_0", "sp_1")
SP_TP = ("sp_0", "sp_1", "tp")
GROUP = ("fs", "tp")
EPS = 1e-06
SOFTMAX_TEMPER = 16.0
HIGH = lax.Precision.HIGHEST


def rms_rows(values, gain):
    mean_square = jnp.mean(values * values, axis=-1, keepdims=True)
    return values * lax.rsqrt(mean_square + EPS) * gain


def own_part(value, at, size, dim):
    return lax.dynamic_slice_in_dim(value, at * size, size, axis=dim)


def combine(earlier, later):
    return (later[1][..., None] * earlier[0] + later[0], earlier[1] * later[1])


def carried_in(value):
    start = (jnp.zeros_like(value[0]), jnp.ones_like(value[1]))
    before, subtotal = start, value
    for axis in ("sp_1", "sp_0"):
        peers, place = lax.axis_size(axis), lax.axis_index(axis)
        both = jnp.concatenate(
            [subtotal[0], jnp.broadcast_to(subtotal[1][..., None], subtotal[0].shape[:-1] + (1,))], -1
        )
        pieces = lax.all_gather(both, axis)
        inside, subtotal = start, start
        for k in range(peers):
            subtotal = combine(subtotal, (pieces[k, ..., :-1], pieces[k, ..., -1]))
            inside = jax.tree.map(lambda n, o: jnp.where(k < place, n, o), subtotal, inside)
        before = combine(inside, before)
    return before[0]


def per_device(
    tokens, norm_gain, gla_query_weight, gla_key_weight, gla_value_weight, decay_down, decay_up,
    decay_bias, head_gain, window_query_weight, window_key_weight, window_value_weight, sink_logit,
    gla_output_weight, window_output_weight,
):
    x = lax.axis_index("fs")
    rows = lax.all_gather(tokens[0], GROUP, axis=0, tiled=True)
    w_in = jnp.concatenate(
        [
            own_part(gla_query_weight, x, 64, 1),
            own_part(gla_key_weight, x, 64, 1),
            own_part(gla_value_weight, x, 128, 1),
            own_part(window_query_weight, x, 128, 1),
            own_part(window_key_weight, x // 2, 64, 1),
            own_part(window_value_weight, x // 2, 64, 1),
            decay_down,
        ],
        axis=1,
    )
    w_in = lax.all_gather(w_in, SP, axis=0, tiled=True)
    w_out = jnp.concatenate(
        [own_part(gla_output_weight, x, 128, 0), own_part(window_output_weight, x, 128, 0)], axis=0
    ).T
    w_out = lax.all_gather(w_out, SP, axis=0, tiled=True)
    normed = rms_rows(rows.astype(jnp.float32), norm_gain).astype(jnp.bfloat16)
    proj = jnp.dot(normed, w_in, preferred_element_type=jnp.float32).astype(jnp.bfloat16)
    seqs = 4
    spans = rows.shape[0] // seqs // SPAN
    gate = jnp.dot(proj[:, 512:], own_part(decay_up, x, 64, 1), preferred_element_type=jnp.float32)
    log_rate = jax.nn.log_sigmoid(gate + own_part(decay_bias, x, 64, 0)) / SOFTMAX_TEMPER

    def blocks(v):
        return v.astype(jnp.float32).reshape(seqs, spans, SPAN, -1)

    q, k, v = blocks(proj[:, :64]) * KEY_DIM**-0.5, blocks(proj[:, 64:128]), blocks(proj[:, 128:256])
    within = jnp.cumsum(blocks(log_rate), axis=2)
    block_total = within[:, :, -1]
    q_dec = q * jnp.exp(within)
    k_dec = k * jnp.exp(-within)
    k_end = k * jnp.exp(block_total[:, :, None] - within)
    scores = jnp.einsum("snid,snjd->snij", q_dec, k_dec, precision=HIGH)
    scores = jnp.where(jnp.tril(jnp.ones((SPAN, SPAN), bool)), scores, 0.0)
    local_out = jnp.einsum("snij,snje->snie", scores, v, precision=HIGH)
    update = jnp.einsum("snjd,snje->snde", k_end, v, precision=HIGH)
    decay = jnp.exp(block_total)
    last_state = decay[:, 1, :, None] * update[:, 0] + update[:, 1]
    incoming = carried_in((last_state, decay[:, 0] * decay[:, 1]))
    entering = jnp.stack([incoming, decay[:, 0, :, None] * incoming + update[:, 0]], axis=1)

    wq = proj[:, 256:384].reshape(seqs, WINDOW, 2, HEAD_DIM)
    wkv = proj[:, 384:512].reshape(seqs, WINDOW, 2 * HEAD_DIM)
    ny, nz = lax.axis_size("sp_1"), lax.axis_size("sp_0")
    n = ny * nz
    edge = lax.ppermute(wkv, SP, [(i, i + 1) for i in range(n - 1)])
    band = jnp.concatenate([edge, wkv], axis=1)
    s = jnp.einsum("sqhd,skd->shqk", wq, band[..., :64], preferred_element_type=jnp.float32)
    s = s * HEAD_DIM**-0.5
    dist = jnp.arange(WINDOW)[:, None] + WINDOW - jnp.arange(2 * WINDOW)[None]
    ok = (dist >= 0) & (dist < WINDOW)
    ok = ok & ((lax.axis_index(SP) > 0) | (jnp.arange(2 * WINDOW)[None] >= WINDOW))
    s = jnp.where(ok, s, -1e30)
    sink = own_part(sink_logit, x, 2, 0)[None, :, None, None]
    top = jnp.maximum(jnp.max(s, -1, keepdims=True), sink)
    e = jnp.exp(s - top)
    den = jnp.sum(e, -1, keepdims=True) + jnp.exp(sink - top)
    att = jnp.einsum(
        "shqk,skd->sqhd", (e / den).astype(jnp.bfloat16), band[..., 64:],
        preferred_element_type=jnp.float32,
    ).astype(jnp.bfloat16)

    gla_out = local_out + jnp.einsum("snid,snde->snie", q_dec, entering, precision=HIGH)
    hidden = rms_rows(gla_out, head_gain).astype(jnp.bfloat16).reshape(-1, VALUE_DIM)
    hidden = jnp.concatenate([hidden, att.reshape(-1, 128)], axis=1)
    total = jnp.einsum("rk,nk->rn", hidden, w_out, preferred_element_type=jnp.float32)
    total = total.astype(jnp.bfloat16).reshape(8, -1, total.shape[1])
    arrived = lax.all_to_all(total, GROUP, split_axis=0, concat_axis=0, tiled=True)
    return arrived.astype(jnp.float32).sum(axis=0).astype(jnp.bfloat16)[None]


def solution(mesh):
    split = Mesh(
        mesh.devices.reshape(8, 8, mesh.shape["fs"], mesh.shape["tp"]), ("sp_0", "sp_1", "fs", "tp")
    )
    return jax.shard_map(
        per_device,
        mesh=split,
        in_specs=(
            P("fs", SP_TP, None), P(), P(SP, "tp"), P(SP, "tp"), P(SP, "tp"), P(SP, None),
            P(None, "tp"), P("tp"), P(), P(SP, "tp"), P(SP, "tp"), P(SP, "tp"), P("tp"),
            P("tp", SP), P("tp", SP),
        ),
        out_specs=P("fs", SP_TP, None),
        check_vma=False,
    )
```

time: 309 us -> 352 us (1.14)
  waiting for transfers between devices: 200 us -> 270 us
  starting transfers between devices: 15.5 us -> 2.84 us
  matrix products: 20.4 us -> 8.02 us
  blocking collectives: 46.2 us -> 35.7 us
  other arithmetic: 7.83 us -> 14.1 us
    all_gather x4 -> x5, waiting for transfers between devices: 198 us -> 268 us  [the longest x1 81.3 us: per_device(): w_in = lax.all_gather(w_in, SP, axis=0, tiled=True)]
    all_gather x2 -> x0, blocking collectives: 37.6 us -> none  [carried_in(): pieces = jax.tree.map(lambda part: lax.all_gather(part, axis), subtotal)]
    all_to_all x1, blocking collectives: 8.59 us -> 35.7 us  [per_device(): lax.all_to_all(total, GROUP, split_axis=0, concat_axis=0, tiled=True)]
    dot_general x15 -> x9, matrix products: 20.4 us -> 8.02 us  [the longest x1 3.24 us: per_device(): jnp.dot(normed, w_in, preferred_element_type=jnp.float32)]
    all_to_all x1 -> x0, starting transfers between devices: 10.3 us -> none  [sent_to_all(): lax.all_to_all(jnp.broadcast_to(value[None], (peers, *value.shape)), axis...]
    dynamic_slice x0 -> x6, local copies, waits for them, and re-layouts: none -> 3.86 us  [own_part(): return lax.dynamic_slice_in_dim(value, at * size, size, axis=dim)]
  transfers between devices with their start and end apart: 7 -> 6, of which waited for: 6 -> 6; matrix products, arithmetic and copies ran while one was open for 5% -> 4% of each run, Pallas kernels for 0% -> 0%
where the time goes in v1:
time: 352 us; the launch traced here: 351 us
  waiting for transfers between devices  270 us (77%)
  blocking collectives  35.7 us (10%)
  other arithmetic  14.1 us (4%)
  between operations  13.5 us (4%)
  matrix products  8.02 us (2%)
  local copies, waits for them, and re-layouts  7.07 us (2%)
    all_gather x1, waiting for transfers between devices, per_device(): w_in = lax.all_gather(w_in, SP, axis=0, tiled=True)  81.3 us
    all_gather x1, waiting for transfers between devices, per_device(): w_out = lax.all_gather(w_out, SP, axis=0, tiled=True)  78.2 us
    all_gather x2, waiting for transfers between devices, carried_in(): pieces = lax.all_gather(both, axis)  74.4 us
    all_to_all x1, blocking collectives, per_device(): lax.all_to_all(total, GROUP, split_axis=0, concat_axis=0, tiled=True)  35.7 us
    all_gather x1, waiting for transfers between devices, per_device(): rows = lax.all_gather(tokens[0], GROUP, axis=0, tiled=True)  34.1 us
  transfers between devices with their start and end apart: 6, of which 6 were waited for; matrix products, arithmetic and copies ran while one was open for 4% of the time, Pallas kernels for 0%

profile of v1, /device:TPU:1, one launch (start us, length us, event | category | flops | bytes accessed | tf_op | source)
XLA Modules:
  0.0 351.1 jit_solution(2613073268380290763)
XLA Ops:
  6.5 0.7 all-gather.13.cloned.1.call-update
  7.3 0.8 constant_dynamic-slice_fusion.2
  8.1 0.8 constant_dynamic-slice_fusion.6
  8.9 0.7 constant_dynamic-slice_fusion.4
  9.6 1.4 concatenate.18
  11.1 0.8 dynamic_slice.40
  11.9 34.1 %all-gather.13.cloned.1.call-done = bf16[1,512,2048]{2,1,0:T(8,128)(2,1)} async-done(((bf16[1,64,2048]{2,1,0:T(8,128)(2,1)}), bf16[1,512,2048]{2,1,0:T(8,128)(2,1)}) %all-gather.13.cloned.1.call-update) | async-done | bytes 2097168 | tf_op jit(solution)/shard_map/all_gather | solution.py:56
  46.0 2.2 fusion
  48.2 81.3 %all-gather.9.cloned.1.call-done = bf16[2048,544]{1,0:T(8,128)(2,1)} async-done(((bf16[32,544]{1,0:T(8,128)(2,1)}), bf16[2048,544]{1,0:T(8,128)(2,1)}) %all-gather.9.cloned.1.call-update) | async-done | bytes 2228240 | tf_op jit(solution)/shard_map/all_gather | solution.py:69
  129.5 3.2 fusion.10
  132.8 0.8 copy-done.3
  133.6 0.4 fusion.28
  133.9 0.1 copy.215
  134.1 0.2 reduce_window_sum.11
  134.3 0.1 copy.197
  134.5 0.1 copy.216
  134.6 0.1 copy.201
  134.7 0.4 fusion.20
  135.1 0.1 fusion.41
  135.3 0.7 pad_maximum_fusion
  136.1 40.0 %all-gather.15.cloned.1.call-done = f32[32,64,129]{2,1,0:T(8,128)} async-done(((f32[4,64,129]{2,1,0:T(8,128)}), f32[32,64,129]{2,1,0:T(8,128)}) %all-gather.15.cloned.1.call-update) | async-done | bytes 1056784 | tf_op jit(solution)/shard_map/all_gather | solution.py:41
  176.1 1.6 slice_reduce_fusion.7
  177.7 1.6 bitcast_add_fusion.9
  179.4 0.7 pad_maximum_fusion.1
  180.2 0.7 constant_dynamic-slice_fusion
  180.9 0.6 maximum_bitcast_fusion
  181.6 0.1 fusion.55
  181.7 0.1 dynamic_slice.41
  181.8 0.9 convert_multiply_fusion.2
  182.6 0.1 copy.214
  182.8 2.7 collective-permute-start
  185.5 0.6 convolution_select_fusion
  186.1 0.3 fusion.64
  186.4 1.0 collective-permute-done
  187.5 0.4 fusion.63
  187.9 0.2 fusion.15
  188.2 0.3 fusion.13
  188.5 0.1 copy.208
  188.6 34.4 %all-gather.17.cloned.1.call-done = f32[32,64,129]{2,1,0:T(8,128)} async-done(((f32[4,64,129]{2,1,0:T(8,128)}), f32[32,64,129]{2,1,0:T(8,128)}) %all-gather.17.cloned.1.call-update) | async-done | bytes 1056784 | tf_op jit(solution)/shard_map/all_gather | solution.py:41
  223.1 1.6 slice_reduce_fusion.6
  224.7 2.0 bitcast_add_fusion
  226.7 0.5 multiply_reduce_fusion
  227.3 0.1 multiply_convert_fusion
  227.4 0.1 copy.209
  227.5 78.2 %all-gather.11.cloned.1.call-done = bf16[2048,256]{1,0:T(8,128)(2,1)} async-done(((bf16[32,256]{1,0:T(8,128)(2,1)}), bf16[2048,256]{1,0:T(8,128)(2,1)}) %all-gather.11.cloned.1.call-update) | async-done | bytes 1048592 | tf_op jit(solution)/shard_map/all_gather | solution.py:73
  305.7 2.0 convolution_convert_fusion
  307.7 35.7 %all_to_all.5 = bf16[8,64,2048]{2,1,0:T(8,128)(2,1)S(1)} all-to-all(bf16[8,64,2048]{2,1,0:T(8,128)(2,1)S(1)} %bitcast.222), channel_id=1, replica_groups=mesh['sp_0'=8,'sp_1'=8,'fs'=4,'tp'=2] {'fs','tp'}, dimensions={0} | all-to-all | bytes 4194304 | tf_op jit(solution)/shard_map/all_to_all | solution.py:125
  343.4 1.1 reduce_sum.42
  (40 shorter events, 0.7 us)
Async XLA Ops:
  6.5 127.0 %copy-start = (bf16[32,256]{1,0:T(8,128)(2,1)S(1)}, bf16[32,256]{1,0:T(8,128)(2,1)}, u32[]{:S(2)}) copy-start(bf16[32,256]{1,0:T(8,128)(2,1)} %param.21) | copy-start | bytes 49156
  6.5 123.0 %copy-start.5 = (f32[2048]{0:T(1024)S(1)}, f32[2048]{0:T(1024)}, u32[]{:S(2)}) copy-start(f32[2048]{0:T(1024)} %param.16) | copy-start | bytes 24580
  6.5 39.5 %all-gather.13.cloned.1.call-start = ((), (), s32[]{:S(2)}) async-start(), calls=%async_computation.3 | async-start | bytes 2359296 | tf_op jit(solution)/shard_map/all_gather | solution.py:56
  7.3 122.2 %all-gather.9.cloned.1.call-start = ((), (), s32[]{:S(2)}) async-start(), calls=%async_computation.1 | async-start | bytes 2662400 | tf_op jit(solution)/shard_map/all_gather | solution.py:69
  11.1 165.0 %all-gather.15.cloned.1.call-start = ((), (), s32[]{:S(2)}) async-start(), calls=%async_computation.4 | async-start | bytes 2359296 | tf_op jit(solution)/shard_map/all_gather | solution.py:41
  46.0 83.5 %copy-start.2 = (bf16[1,512,2048]{2,1,0:T(8,128)(2,1)S(1)}, bf16[1,512,2048]{2,1,0:T(8,128)(2,1)}, u32[]{:S(2)}) copy-start(bf16[1,512,2048]{2,1,0:T(8,128)(2,1)} %all-gather.13.cloned.1.call-done) | copy-start | bytes 6291460
  132.8 0.8 copy-start.3
  135.2 46.5 %copy-start.6 = (f32[8]{0:T(128)S(1)}, f32[8]{0:T(128)}, u32[]{:S(2)}) copy-start(f32[8]{0:T(128)} %param.27) | copy-start | bytes 100
  136.0 87.1 %all-gather.17.cloned.1.call-start = ((), (), s32[]{:S(2)}) async-start(), calls=%async_computation.5 | async-start | bytes 2359296 | tf_op jit(solution)/shard_map/all_gather | solution.py:41
  180.1 125.6 %all-gather.11.cloned.1.call-start = ((), (), s32[]{:S(2)}) async-start(), calls=%async_computation.2 | async-start | bytes 1064960 | tf_op jit(solution)/shard_map/all_gather | solution.py:73
  182.8 4.6 %collective-permute-start = (bf16[4,128,128]{1,2,0:T(8,128)(2,1)S(1)}, bf16[4,128,128]{1,2,0:T(8,128)(2,1)S(1)}, u32[]{:S(2)}, u32[]{:S(2)}) collective-permute-start(bf16[4,128,128]{1,2,0:T(8,128)(2,1)S(1)} %bitcast.238), channel_id=1, source_target_pairs={{0,8},{8,16},{16,24},{24,32},{32,40},{40,48},{48,56},{56,64},{64,7... | collective-permute-start | bytes 393224 | tf_op jit(solution)/shard_map/ppermute | solution.py:103
  188.2 36.6 %copy-start.1 = (f32[32,64,129]{2,1,0:T(8,128)S(1)}, f32[32,64,129]{2,1,0:T(8,128)}, u32[]{:S(2)}) copy-start(f32[32,64,129]{2,1,0:T(8,128)} %all-gather.15.cloned.1.call-done) | copy-start | bytes 3170308
  224.7 2.5 copy-start.4
Sparse Core Ops, SparseCore 0:
  9.5 36.4 all-gather.12
  49.0 80.4 all-gather.8
  136.1 39.8 all-gather.14
  180.2 42.7 all-gather.16
  226.0 79.6 all-gather.10

commit v2 on v1

v2 whole, which is shorter than its diff:
```python
import functools

import jax
import jax.numpy as jnp
from jax import lax
from jax.experimental import pallas as pl
from jax.experimental.pallas import tpu as pltpu
from jax.sharding import Mesh
from jax.sharding import PartitionSpec as P

F32, BF16 = jnp.float32, jnp.bfloat16
MESH = pl.DeviceIdType.MESH
HIGH = lax.Precision.HIGHEST
SP = ("sp_0", "sp_1")
SP_TP = ("sp_0", "sp_1", "tp")
EPS = 1e-06
N = 8
SEQS = 4
D = 2048
PARTS = ((0, 5, "sp_1", "sp_0"), (5, 9, "sp_0", "sp_1"), (9, 11, "sp_1", "sp_0"), (11, 13, "sp_0", "sp_1"))


def dot(a, b, contract=((1,), (0,)), precision=None):
    return lax.dot_general(
        a, b, (contract, ((), ())), precision=precision, preferred_element_type=F32
    )


def wrap(i, n=N):
    return lax.rem(i + 4 * n, n)


def kernel(
    tokens, norm_gain, gq, gk, gv, decay_down, decay_up, decay_bias, head_gain, wq, wk, wv,
    sink, go, wo, out,
    W, T, normed, kv, edge, state, got1, tot, got2, ret, enter, take, hop, hopin, fin, finin,
    w_send, w_recv, t_send, t_recv, p_send, p_recv, e_sem, s_send, s_recv, o_send, o_recv,
    x_send, x_recv,
):
    z, y = lax.axis_index("sp_0"), lax.axis_index("sp_1")
    x, c = lax.axis_index("fs"), lax.axis_index("tp")
    me = z * N + y
    at = {"sp_0": z, "sp_1": y}
    right, left, across = wrap(x + 1, 4), wrap(x - 1, 4), wrap(x + 2, 4)
    partner = {"tp": 1 - c}
    after, before = wrap(me + 1, 64), wrap(me - 1, 64)
    after_id = {"sp_0": after // N, "sp_1": lax.rem(after, N)}
    before_id = {"sp_0": before // N, "sp_1": lax.rem(before, N)}

    barrier = pltpu.get_barrier_semaphore()

    def greet(device_id):
        pl.semaphore_signal(barrier, inc=1, device_id=device_id, device_id_type=MESH)

    for name in SP:
        for d in range(1, N):
            greet({name: wrap(at[name] + d)})
    greet({"fs": right})
    greet({"fs": left})
    greet(partner)
    greet(after_id)
    greet(before_id)

    def pick(ref, width, index, count):
        got = ref[:, 0:width]
        for i in range(1, count):
            got = jnp.where(index == i, ref[:, i * width : (i + 1) * width], got)
        return got

    def put(block, value):
        W[me, block] = value[0:16]
        W[me, block + 1] = value[16:32]

    put(0, jnp.concatenate([pick(gq, 64, x, 4), pick(gk, 64, x, 4)], axis=1))
    put(2, pick(gv, 128, x, 4))
    down = decay_down[...]
    W[me, 4] = jnp.concatenate([down[0:16], down[16:32], jnp.zeros((16, 64), BF16)], axis=1)
    put(5, pick(wq, 128, x, 4))
    put(7, jnp.concatenate([pick(wk, 64, x // 2, 2), pick(wv, 64, x // 2, 2)], axis=1))
    eye = (
        lax.broadcasted_iota(jnp.int32, (32, 32), 0) == lax.broadcasted_iota(jnp.int32, (32, 32), 1)
    ).astype(BF16)
    own_rows = pl.ds(pl.multiple_of(x * 128, 128), 128)
    put(9, dot(eye, go[own_rows, :], ((1,), (1,))).astype(BF16))
    put(11, dot(eye, wo[own_rows, :], ((1,), (1,))).astype(BF16))
    for q in range(4):
        T[x, c, q] = tokens[q]

    pl.semaphore_wait(barrier, 2 * (N - 1) + 5)

    def piece(part, shard, device_id):
        a, b, _, _ = PARTS[part]
        ref = W.at[shard, a:b]
        return pltpu.make_async_remote_copy(
            src_ref=ref, dst_ref=ref, send_sem=w_send.at[part], recv_sem=w_recv.at[part, shard],
            device_id=device_id, device_id_type=MESH,
        )

    def first_hop(part):
        name = PARTS[part][2]
        for d in (1, 7, 2, 6, 3, 5, 4):
            piece(part, me, {name: wrap(at[name] + d)}).start()

    def ring_step(part, h, j):
        _, _, near, far = PARTS[part]
        offset = ((j + 1) // 2) * (2 * lax.rem(j, 2) - 1)
        line = wrap(at[near] + offset)
        up, down_ = {far: wrap(at[far] + 1)}, {far: wrap(at[far] - 1)}

        def shard(across_by):
            spot = wrap(at[far] + across_by)
            return line * N + spot if near == "sp_0" else spot * N + line

        def arrive(s):
            piece(part, s, up).wait_recv()

        if h == 0:
            s = shard(0)
            pl.when(j > 0)(lambda: arrive(s))
            piece(part, s, up).start()
            piece(part, s, down_).start()
        elif h < 3:
            s = shard(-h)
            arrive(s)
            piece(part, s, up).start()
            s = shard(h)
            arrive(s)
            piece(part, s, down_).start()
        elif h == 3:
            s, r = shard(-3), shard(3)
            arrive(s)
            pl.when(j < 4)(lambda: piece(part, s, up).start())
            arrive(r)
            pl.when(j >= 4)(lambda: piece(part, r, down_).start())
        else:
            arrive(shard(4))

    def ring(parts, h, more=None):
        def body(j, carry):
            for part in parts:
                ring_step(part, h, j)
            if more is not None:
                more(j)
            return carry

        lax.fori_loop(0, N, body, 0)

    def chunk(seq, q, device_id, own=False):
        return pltpu.make_async_remote_copy(
            src_ref=tokens.at[q] if own else T.at[seq, c, q], dst_ref=T.at[seq, c, q],
            send_sem=t_send, recv_sem=t_recv.at[seq, q], device_id=device_id, device_id_type=MESH,
        )

    def twin(seq, q, own=False):
        return pltpu.make_async_remote_copy(
            src_ref=tokens.at[q] if own else T.at[seq, c, q], dst_ref=T.at[seq, c, q],
            send_sem=p_send, recv_sem=p_recv.at[seq, q], device_id=partner, device_id_type=MESH,
        )

    def tokens_step(i):
        if i < 4:
            arrivals = ((left, i, right), (right, (i + 2) % 4, left))
        else:
            arrivals = ((across, i - 4, None), (across, i - 2, None))
        for seq, q, onward in arrivals:
            chunk(seq, q, partner).wait_recv()
            if i < 2:
                chunk(seq, q, {"fs": onward}).start()
            twin(seq, q).start()

    for i in range(4):
        chunk(x, i, {"fs": right}, True).start()
        chunk(x, (i + 2) % 4, {"fs": left}, True).start()
    first_hop(0)
    first_hop(1)
    for q in range(4):
        twin(x, q, True).start()
    first_hop(2)
    first_hop(3)
    tokens_step(0)
    tokens_step(1)
    ring((0, 1), 0)
    tokens_step(2)
    tokens_step(3)
    ring((0, 1), 1)
    tokens_step(4)
    tokens_step(5)
    for seq in range(SEQS):
        for q in range(4):
            pltpu.make_async_remote_copy(
                src_ref=T.at[seq, 1 - c, q], dst_ref=T.at[seq, 1 - c, q], send_sem=p_send,
                recv_sem=p_recv.at[seq, q], device_id=partner, device_id_type=MESH,
            ).wait_recv()

    def norm_rows(j, offset):
        index = 2 * j + offset
        seq, half = index // 8, lax.rem(index // 4, 2)
        q = lax.rem(index, 4)
        rows = T[seq, half, q].astype(F32)
        mean_square = jnp.mean(rows * rows, axis=-1, keepdims=True)
        rows = rows * lax.rsqrt(mean_square + EPS) * norm_gain[...]
        normed[pl.ds(pl.multiple_of(index * 16, 16), 16), :] = rows.astype(BF16)

    def norm_two(base):
        def more(j):
            norm_rows(j, base)
            norm_rows(j, base + 1)

        return more

    ring((0, 1), 2, norm_two(0))
    ring((0, 1), 3, norm_two(16))
    ring((0,), 4)

    def tile(block):
        return W[:, block : block + 2].reshape(D, 128)

    rows = normed[...]
    lane = lax.broadcasted_iota(jnp.int32, (64, 16, 128), 2)
    low = W[:, 4]
    zero = jnp.zeros_like(low)
    low = jnp.stack([jnp.where(lane < 32, low, zero), jnp.where(lane >= 32, low, zero)], axis=1)
    low = dot(rows, low.reshape(D, 128))
    low_rank = (low[:, 0:32] + low[:, 32:64]).astype(BF16)
    proj = dot(rows, jnp.concatenate([tile(0), tile(2)], axis=1))
    gate = dot(low_rank, pick(decay_up, 64, x, 4)) + pick(decay_bias, 64, x, 4)
    u = jnp.exp(-jnp.abs(gate))
    log1p = jnp.where(u < 0.01, u * (1.0 - u * (0.5 - u * (1.0 / 3.0))), jnp.log(1.0 + u))
    log_rate = (jnp.minimum(gate, 0.0) - log1p) / 16.0
    query = proj[:, 0:64].astype(BF16).astype(F32) * 64**-0.5
    key = proj[:, 64:128].astype(BF16).astype(F32)
    value = proj[:, 128:256].astype(BF16).astype(F32)

    lower = lax.broadcasted_iota(jnp.int32, (64, 64), 0) >= lax.broadcasted_iota(jnp.int32, (64, 64), 1)
    ones = lower.astype(F32)
    spans = [slice(64 * i, 64 * (i + 1)) for i in range(2 * SEQS)]
    within = [dot(ones, log_rate[r], precision=HIGH) for r in spans]
    totals = [w[63:64] for w in within]
    column = [jnp.transpose(jnp.broadcast_to(t, (128, 64))) for t in totals]
    update = [
        dot(jnp.transpose(key[r] * jnp.exp(t - w)), value[r], precision=HIGH)
        for r, w, t in zip(spans, within, totals)
    ]
    for seq in range(SEQS):
        a, b = 2 * seq, 2 * seq + 1
        last = jnp.exp(column[b]) * update[a] + update[b]
        fall = column[a] + column[b]
        for half in range(2):
            part = slice(32 * half, 32 * (half + 1))
            state[a + half, 0] = last[part].astype(BF16)
            state[a + half, 1] = fall[part].astype(BF16)

    def spread(stage, name, src, dst):
        place = at[name]
        for d in (4, 3, 5, 2, 6, 1, 7):
            peer = wrap(place + d)
            pltpu.make_async_remote_copy(
                src_ref=src(peer), dst_ref=dst.at[place], send_sem=s_send.at[stage, d],
                recv_sem=s_recv.at[stage, place], device_id={name: peer}, device_id_type=MESH,
            ).start()

    def spread_wait(stage, name, src, dst):
        place = at[name]
        for d in (1, 7, 2, 6, 3, 5, 4):
            peer = wrap(place + d)
            pltpu.make_async_remote_copy(
                src_ref=src(peer), dst_ref=dst.at[peer], send_sem=s_send.at[stage, d],
                recv_sem=s_recv.at[stage, peer], device_id={name: peer}, device_id_type=MESH,
            ).wait()

    spread(0, "sp_1", lambda i: state.at[i], got1)
    got1[y] = state[y]

    ring((1,), 4)
    wproj = dot(rows, jnp.concatenate([tile(5), tile(7)], axis=1)).astype(BF16)
    for seq in range(SEQS):
        kv[seq] = wproj[128 * seq : 128 * (seq + 1), 128:256]

    q_dec = [query[r] * jnp.exp(w) for r, w in zip(spans, within)]
    edge_copy = pltpu.make_async_remote_copy(
        src_ref=kv, dst_ref=edge, send_sem=e_sem.at[0], recv_sem=e_sem.at[1],
        device_id=after_id, device_id_type=MESH,
    )
    edge_copy.start()

    local = []
    for r, w, qd in zip(spans, within, q_dec):
        scores = dot(qd, key[r] * jnp.exp(-w), ((1,), (1,)), HIGH)
        local.append(dot(jnp.where(lower, scores, 0.0), value[r], precision=HIGH))

    spread_wait(0, "sp_1", lambda i: state.at[i], got1)
    run = jnp.zeros((32, 128), F32)
    fall = jnp.zeros((32, 128), F32)
    prefix, falls = [], []
    for i in range(N):
        prefix.append(run)
        falls.append(fall)
        step = got1[i, 1].astype(F32)
        run = jnp.exp(step) * run + got1[i, 0].astype(F32)
        fall = fall + step
    tot[0] = run.astype(BF16)
    tot[1] = fall.astype(BF16)
    spread(1, "sp_0", lambda i: tot, got2)
    got2[z] = tot[...]

    ring((2, 3), 0)
    ring((2, 3), 1)
    spread_wait(1, "sp_0", lambda i: tot, got2)
    come = jnp.zeros((32, 128), F32)
    for i in range(N):
        come = jnp.where(
            i < z, jnp.exp(got2[i, 1].astype(F32)) * come + got2[i, 0].astype(F32), come
        )
    for i in range(N):
        ret[i] = (jnp.exp(falls[i]) * come + prefix[i]).astype(BF16)
    spread(2, "sp_1", lambda i: ret.at[i], enter)
    enter[y] = ret[y]

    ring((2, 3), 2)
    edge_copy.wait()
    distance = (
        lax.broadcasted_iota(jnp.int32, (128, 256), 0)
        + 128
        - lax.broadcasted_iota(jnp.int32, (128, 256), 1)
    )
    first_key = jnp.where(me > 0, 0, 128)
    valid = (distance >= 0) & (distance < 128)
    valid = valid & (lax.broadcasted_iota(jnp.int32, (128, 256), 1) >= first_key)
    sinks = pick(sink, 2, x, 4)
    window = []
    for seq in range(SEQS):
        band = jnp.concatenate([edge[seq], kv[seq]], axis=0)
        heads = []
        for head in range(2):
            qh = wproj[128 * seq : 128 * (seq + 1), 64 * head : 64 * (head + 1)]
            s = dot(qh, band[:, 0:64], ((1,), (1,))) * 64**-0.5
            s = jnp.where(valid, s, -1e30)
            sink_term = sinks[:, head : head + 1]
            top = jnp.maximum(jnp.max(s, axis=-1, keepdims=True), sink_term)
            expo = jnp.exp(s - top)
            denom = jnp.sum(expo, axis=-1, keepdims=True) + jnp.exp(sink_term - top)
            heads.append(dot((expo / denom).astype(BF16), band[:, 64:128]))
        window.append(jnp.concatenate(heads, axis=1).astype(BF16))
        if seq == 1:
            ring((2, 3), 3)
    ring((2, 3), 4)

    spread_wait(2, "sp_1", lambda i: ret.at[i], enter)
    hidden = []
    for seq in range(SEQS):
        a, b = 2 * seq, 2 * seq + 1
        come = jnp.concatenate([enter[a], enter[b]], axis=0).astype(F32)
        middle = jnp.exp(column[a]) * come + update[a]
        for i, entering in ((a, come), (b, middle)):
            gla = local[i] + dot(q_dec[i], entering, precision=HIGH)
            mean_square = jnp.mean(gla * gla, axis=-1, keepdims=True)
            hidden.append((gla * lax.rsqrt(mean_square + EPS) * head_gain[...]).astype(BF16))

    out_map = jnp.concatenate([tile(9), tile(11)], axis=1)

    def total(seq_static):
        h = jnp.concatenate(hidden[2 * seq_static : 2 * seq_static + 2], axis=0)
        return dot(jnp.concatenate([h, window[seq_static]], axis=1), out_map, ((1,), (1,)))

    for seq in range(SEQS):
        t = total(seq)
        normed[128 * seq : 128 * (seq + 1), :] = t.astype(BF16)

    def to_partner(seq):
        return pltpu.make_async_remote_copy(
            src_ref=normed.at[pl.ds(pl.multiple_of(seq * 128 + (1 - c) * 64, 64), 64), :],
            dst_ref=take.at[seq], send_sem=o_send.at[seq], recv_sem=o_recv.at[seq],
            device_id=partner, device_id_type=MESH,
        )

    for seq in (across, right, left, x):
        to_partner(seq).start()

    def chip_sum(seq):
        to_partner(seq).wait_recv()
        own = normed[pl.ds(pl.multiple_of(seq * 128 + c * 64, 64), 64), :]
        return own.astype(F32) + take[seq].astype(F32)

    def move(index, src, dst, device_id):
        return pltpu.make_async_remote_copy(
            src_ref=src, dst_ref=dst, send_sem=x_send.at[index], recv_sem=x_recv.at[index],
            device_id={"fs": device_id}, device_id_type=MESH,
        )

    s = chip_sum(across).astype(BF16)
    hop[0] = s[:, 0:1024]
    hop[1] = s[:, 1024:2048]
    moves = [move(0, hop.at[0], hopin.at[0], right), move(1, hop.at[1], hopin.at[1], left)]
    moves[0].start()
    moves[1].start()
    to_right = chip_sum(right)
    fin[1] = to_right[:, 1024:2048].astype(BF16)
    moves.append(move(2, fin.at[1], finin.at[1], right))
    moves[2].start()
    to_left = chip_sum(left)
    fin[2] = to_left[:, 0:1024].astype(BF16)
    moves.append(move(3, fin.at[2], finin.at[2], left))
    moves[3].start()
    moves[0].wait_recv()
    fin[0] = (to_right[:, 0:1024] + hopin[0].astype(F32)).astype(BF16)
    moves.append(move(4, fin.at[0], finin.at[0], right))
    moves[4].start()
    moves[1].wait_recv()
    fin[3] = (to_left[:, 1024:2048] + hopin[1].astype(F32)).astype(BF16)
    moves.append(move(5, fin.at[3], finin.at[3], left))
    moves[5].start()
    mine = chip_sum(x)
    for i in (2, 3, 4, 5):
        moves[i].wait_recv()
    low_half = mine[:, 0:1024] + finin[0].astype(F32) + finin[2].astype(F32)
    high_half = mine[:, 1024:2048] + finin[1].astype(F32) + finin[3].astype(F32)
    out[:, 0:1024] = low_half.astype(BF16)
    out[:, 1024:2048] = high_half.astype(BF16)

    for i in range(6):
        moves[i].wait_send()
    for seq in range(SEQS):
        to_partner(seq).wait_send()
    for part in range(4):
        a, b, _, _ = PARTS[part]
        ref = W.at[0:63, a:b]
        pltpu.make_async_copy(ref, ref, w_send.at[part]).wait()
    ref = T.at[0:3, 0]
    pltpu.make_async_copy(ref, ref, t_send).wait()
    ref = T.at[0:4, 0]
    pltpu.make_async_copy(ref, ref, p_send).wait()


def per_device(
    tokens, norm_gain, gla_query_weight, gla_key_weight, gla_value_weight, decay_down, decay_up,
    decay_bias, head_gain, window_query_weight, window_key_weight, window_value_weight, sink_logit,
    gla_output_weight, window_output_weight,
):
    dma, vmem = pltpu.SemaphoreType.DMA, pltpu.VMEM
    return pl.pallas_call(
        kernel,
        out_shape=jax.ShapeDtypeStruct((64, D), BF16),
        in_specs=[pl.BlockSpec(memory_space=pltpu.VMEM)] * 15,
        out_specs=pl.BlockSpec(memory_space=pltpu.VMEM),
        scratch_shapes=[
            vmem((64, 13, 16, 128), BF16),
            vmem((4, 2, 4, 16, D), BF16),
            vmem((512, D), BF16),
            vmem((4, 128, 128), BF16),
            vmem((4, 128, 128), BF16),
            vmem((N, 2, 32, 128), BF16),
            vmem((N, 2, 32, 128), BF16),
            vmem((2, 32, 128), BF16),
            vmem((N, 2, 32, 128), BF16),
            vmem((N, 32, 128), BF16),
            vmem((N, 32, 128), BF16),
            vmem((4, 64, D), BF16),
            vmem((2, 64, 1024), BF16),
            vmem((2, 64, 1024), BF16),
            vmem((4, 64, 1024), BF16),
            vmem((4, 64, 1024), BF16),
            dma((4,)),
            dma((4, 64)),
            dma,
            dma((4, 4)),
            dma,
            dma((4, 4)),
            dma((2,)),
            dma((3, N)),
            dma((3, N)),
            dma((4,)),
            dma((4,)),
            dma((6,)),
            dma((6,)),
        ],
        compiler_params=pltpu.CompilerParams(
            collective_id=0, has_side_effects=True, vmem_limit_bytes=48 * 1024 * 1024
        ),
    )(
        tokens.reshape(4, 16, D),
        norm_gain.reshape(1, D),
        gla_query_weight,
        gla_key_weight,
        gla_value_weight,
        decay_down,
        decay_up,
        decay_bias.reshape(1, -1),
        head_gain.reshape(1, -1),
        window_query_weight,
        window_key_weight,
        window_value_weight,
        sink_logit.reshape(1, -1),
        gla_output_weight,
        window_output_weight,
    )[None]


def solution(mesh):
    split = Mesh(
        mesh.devices.reshape(N, N, mesh.shape["fs"], mesh.shape["tp"]), ("sp_0", "sp_1", "fs", "tp")
    )
    return jax.shard_map(
        per_device,
        mesh=split,
        in_specs=(
            P("fs", SP_TP, None), P(), P(SP, "tp"), P(SP, "tp"), P(SP, "tp"), P(SP, None),
            P(None, "tp"), P("tp"), P(), P(SP, "tp"), P(SP, "tp"), P(SP, "tp"), P("tp"),
            P("tp", SP), P("tp", SP),
        ),
        out_specs=P("fs", SP_TP, None),
        check_vma=False,
    )
```

time: 352 us -> 88.1 us (0.25)
  waiting for transfers between devices: 270 us -> 0 us
  Pallas kernels: 0 us -> 79.3 us
  blocking collectives: 35.7 us -> 0 us
  other arithmetic: 14.1 us -> 0 us
  between operations: 13.5 us -> 0.1 us
  matrix products: 8.02 us -> 0 us
    all_gather x5 -> x0, waiting for transfers between devices: 268 us -> none  [the longest x1 81.3 us: per_device(): w_in = lax.all_gather(w_in, SP, axis=0, tiled=True)]
    pallas_call x0 -> x1, Pallas kernels: none -> 79.3 us  [per_device(): pl.pallas_call(kernel, out_shape=jax.ShapeDtypeStruct((64, D), BF16), in_...]
    all_to_all x1 -> x0, blocking collectives: 35.7 us -> none  [per_device(): lax.all_to_all(total, GROUP, split_axis=0, concat_axis=0, tiled=True)]
    dot_general x9 -> x0, matrix products: 8.02 us -> none  [the longest x1 3.24 us: per_device(): jnp.dot(normed, w_in, preferred_element_type=jnp.float32)]
    unnamed x16 -> x29, local copies, waits for them, and re-layouts: 0.83 us -> 8.1 us
    dynamic_slice x6 -> x0, local copies, waits for them, and re-layouts: 3.86 us -> none  [own_part(): return lax.dynamic_slice_in_dim(value, at * size, size, axis=dim)]
    add x5 -> x0, other arithmetic: 3.78 us -> none  [the longest x1 1.97 us: per_device(): decay[:, 0, :, None] * incoming + update[:, 0]]
  transfers between devices with their start and end apart: 6 -> 0, of which waited for: 6 -> 0; matrix products, arithmetic and copies ran while one was open for 4% -> 0% of each run, Pallas kernels for 0% -> 0%
where the time goes in v2:
time: 88.1 us; the launch traced here: 87.5 us
  Pallas kernels  79.3 us (90%)
  local copies, waits for them, and re-layouts  8.1 us (9%)
    pallas_call x1, Pallas kernels, per_device(): pl.pallas_call(kernel, out_shape=jax.ShapeDtypeStruct((64, D), BF16), in_...  79.3 us
    unnamed x29, local copies, waits for them, and re-layouts  8.1 us

profile of v2, /device:TPU:1, one launch (start us, length us, event | category | flops | bytes accessed | tf_op | source)
XLA Modules:
  0.0 87.5 jit_solution(11748899456103402716)
XLA Ops:
  0.0 0.0 copy-start
  0.0 0.9 %copy.16.go = bf16[512,32]{1,0:T(8,128)(2,1)S(1)} copy(bf16[512,32]{0,1:T(8,128)(2,1)} %param.28) | data formatting | bytes 65536 | tf_op args[13]
  0.9 0.0 copy-start.1
  0.9 0.0 copy-start.2
  0.9 0.0 copy-start.6
  1.0 0.0 copy-start.10
  1.0 0.9 %copy.17.wo = bf16[512,32]{1,0:T(8,128)(2,1)S(1)} copy(bf16[512,32]{0,1:T(8,128)(2,1)} %param.29) | data formatting | bytes 65536 | tf_op args[14]
  1.9 0.0 copy-done
  1.9 0.0 copy-done.1
  1.9 0.0 copy-done.2
  1.9 0.0 copy-done.6
  1.9 0.0 copy-done.10
  1.9 0.0 copy-start.3
  1.9 0.7 copy-done.3
  2.6 0.0 copy-start.4
  2.6 0.7 copy-done.4
  3.4 0.0 copy-start.5
  3.4 0.7 copy-done.5
  4.1 0.0 copy-start.7
  4.1 0.7 copy-done.7
  4.8 0.0 copy-start.8
  4.8 0.7 copy-done.8
  5.5 0.0 copy-start.9
  5.5 0.7 copy-done.9
  6.2 0.0 copy-start.11
  6.2 0.7 copy-done.11
  6.8 0.0 copy-start.12
  6.8 0.7 copy-done.12
  7.5 79.3 %shard_map.145 = bf16[64,2048]{1,0:T(8,128)(2,1)S(1)} custom-call(bf16[4,16,2048]{2,1,0:T(8,128)(2,1)S(1)} %bitcast.7, f32[1,2048]{1,0:T(1,128)S(1)} %bitcast.8, bf16[32,256]{1,0:T(8,128)(2,1)S(1)} %copy-done.3, bf16[32,256]{1,0:T(8,128)(2,1)S(1)} %copy-done.4, bf16[32,512]{1,0:T(8,128)(2,1)S(1)} %copy-done.1, bf16[32,32]{1,0:T(8,128)(2,1)S(1)} %copy-done.7, ...), custom_call_target="tpu_custom_call" | custom-call | tf_op jit(solution)/shard_map/pallas_call | solution.py:440
  86.8 0.7 copy.19
Async XLA Ops:
  0.0 1.9 %copy-start = (bf16[1,64,2048]{2,1,0:T(8,128)(2,1)S(1)}, bf16[1,64,2048]{2,1,0:T(8,128)(2,1)}, u32[]{:S(2)}) copy-start(bf16[1,64,2048]{2,1,0:T(8,128)(2,1)} %param.15) | copy-start | bytes 786436
  0.9 1.0 %copy-start.1 = (bf16[32,512]{1,0:T(8,128)(2,1)S(1)}, bf16[32,512]{1,0:T(8,128)(2,1)}, u32[]{:S(2)}) copy-start(bf16[32,512]{1,0:T(8,128)(2,1)} %gv.1) | copy-start | bytes 98308
  0.9 1.0 %copy-start.2 = (bf16[32,512]{1,0:T(8,128)(2,1)S(1)}, bf16[32,512]{1,0:T(8,128)(2,1)}, u32[]{:S(2)}) copy-start(bf16[32,512]{1,0:T(8,128)(2,1)} %wq.1) | copy-start | bytes 98308
  0.9 1.0 %copy-start.6 = (f32[2048]{0:T(1024)S(1)}, f32[2048]{0:T(1024)}, u32[]{:S(2)}) copy-start(f32[2048]{0:T(1024)} %param.16) | copy-start | bytes 24580
  1.0 1.0 %copy-start.10 = (f32[256]{0:T(256)S(1)}, f32[256]{0:T(256)}, u32[]{:S(2)}) copy-start(f32[256]{0:T(256)} %param.22) | copy-start | bytes 3076
  1.9 0.7 copy-start.3
  2.6 0.7 copy-start.4
  3.4 0.7 copy-start.5
  4.1 0.7 copy-start.7
  4.8 0.7 copy-start.8
  5.5 0.7 copy-start.9
  6.2 0.7 copy-start.11
  6.8 0.7 copy-start.12

commit v3 on v2

v3 whole, which is shorter than its diff:
```python
import contextlib

import jax
import jax.numpy as jnp
from jax import lax
from jax.experimental import pallas as pl
from jax.experimental.pallas import tpu as pltpu
from jax.sharding import Mesh
from jax.sharding import PartitionSpec as P

F32, BF16 = jnp.float32, jnp.bfloat16
MESH = pl.DeviceIdType.MESH
HIGH = lax.Precision.HIGHEST
SP = ("sp_0", "sp_1")
SP_TP = ("sp_0", "sp_1", "tp")
EPS = 1e-06
N = 8
SEQS = 4
D = 2048
PARTS = ((0, 5, "sp_1", "sp_0"), (5, 9, "sp_0", "sp_1"), (9, 11, "sp_1", "sp_0"), (11, 13, "sp_0", "sp_1"))


def dot(a, b, contract=((1,), (0,)), precision=None):
    return lax.dot_general(
        a, b, (contract, ((), ())), precision=precision, preferred_element_type=F32
    )


def wrap(i, n=N):
    return lax.rem(i + n, n)


def kernel(*refs):
    sources, out, places = refs[:15], refs[15], refs[16:31]
    (
        in_sems, W, T, normed, acc, kv, edge, state, got1, tot, got2, ret, enter, hid, whole, take,
        hop, hopin, fin, finin, w_send, w_line, w_far, o_line, o_far, t_send, t_recv, p_send,
        p_recv, e_sem, s_send, s_recv, o_send, o_recv, x_send, x_recv,
    ) = refs[31:]
    (
        tokens, norm_gain, gq, gk, gv, decay_down, decay_up, decay_bias, head_gain, wq, wk, wv,
        sink, go, wo,
    ) = places
    scope = contextlib.ExitStack()

    def phase(name):
        scope.close()
        scope.enter_context(jax.named_scope(name))

    phase("greet")
    z, y = lax.axis_index("sp_0"), lax.axis_index("sp_1")
    x, c = lax.axis_index("fs"), lax.axis_index("tp")
    me = z * N + y
    at = {"sp_0": z, "sp_1": y}
    right, left, across = wrap(x + 1, 4), wrap(x - 1, 4), wrap(x + 2, 4)
    partner = {"tp": 1 - c}
    after, before = wrap(me + 1, 64), wrap(me - 1, 64)
    after_id = {"sp_0": after // N, "sp_1": lax.rem(after, N)}
    before_id = {"sp_0": before // N, "sp_1": lax.rem(before, N)}

    barrier = pltpu.get_barrier_semaphore()

    def greet(device_id):
        pl.semaphore_signal(barrier, inc=1, device_id=device_id, device_id_type=MESH)

    for name in SP:
        for d in (4, 3, 5, 2, 6, 1, 7):
            greet({name: wrap(at[name] + d)})
    greet(after_id)
    greet(before_id)
    greet({"fs": right})
    greet({"fs": left})
    greet(partner)

    phase("inputs")
    for i in range(15):
        pltpu.make_async_copy(sources[i], places[i], in_sems.at[i]).start()
    for i in range(15):
        pltpu.make_async_copy(sources[i], places[i], in_sems.at[i]).wait()

    phase("pack")

    def pick(ref, width, index, count):
        got = ref[:, 0:width]
        for i in range(1, count):
            got = jnp.where(index == i, ref[:, i * width : (i + 1) * width], got)
        return got

    def put(block, value):
        W[z, y, block] = value[0:16]
        W[z, y, block + 1] = value[16:32]

    put(0, jnp.concatenate([pick(gq, 64, x, 4), pick(gk, 64, x, 4)], axis=1))
    put(2, pick(gv, 128, x, 4))
    down = decay_down[...]
    W[z, y, 4] = jnp.concatenate([down[0:16], down[16:32], jnp.zeros((16, 64), BF16)], axis=1)
    put(5, pick(wq, 128, x, 4))
    put(7, jnp.concatenate([pick(wk, 64, x // 2, 2), pick(wv, 64, x // 2, 2)], axis=1))
    put(9, pick(go, 128, x, 4))
    put(11, pick(wo, 128, x, 4))

    def norm_rows(seq, half, source=None):
        def body(q, carry):
            rows = (T[seq, half, q] if source is None else source[q]).astype(F32)
            mean_square = jnp.mean(rows * rows, axis=-1, keepdims=True)
            rows = rows * lax.rsqrt(mean_square + EPS) * norm_gain[...]
            index = (seq * 8 + half * 4 + q) * 16
            normed[pl.ds(pl.multiple_of(index, 16), 16), :] = rows.astype(BF16)
            return carry

        lax.fori_loop(0, 4, body, 0)

    norm_rows(x, c, tokens)
    phase("barrier")
    pl.semaphore_wait(barrier, 2 * (N - 1) + 5)

    def region(part, far_spot, line_spot, count):
        a, b, near, _ = PARTS[part]
        line = pl.ds(line_spot, count)
        return W.at[far_spot, line, a:b] if near == "sp_1" else W.at[line, far_spot, a:b]

    def send(part, ref, recv_sem, device_id):
        return pltpu.make_async_remote_copy(
            src_ref=ref, dst_ref=ref, send_sem=w_send.at[part], recv_sem=recv_sem,
            device_id=device_id, device_id_type=MESH,
        )

    def first_hop(part):
        _, _, near, far = PARTS[part]
        ref = region(part, at[far], at[near], 1)
        sem = w_line.at[part, at[near]] if part < 2 else o_line.at[part - 2]
        for d in (1, 7, 2, 6, 3, 5, 4):
            send(part, ref, sem, {near: wrap(at[near] + d)}).start()

    def ring_step(part, h, j):
        _, _, near, far = PARTS[part]
        up, down_ = {far: wrap(at[far] + 1)}, {far: wrap(at[far] - 1)}
        if part < 2:
            group = wrap(at[near] // 2 + (0, 1, -1, 2)[j], 4)
            count, groups, sems = 2, 4, w_far.at[part]
        else:
            group = j
            count, groups, sems = 4, 2, o_far.at[part - 2]

        def leg(far_by, device_id):
            spot = wrap(at[far] + far_by)
            return send(
                part, region(part, spot, group * count, count), sems.at[spot, group], device_id
            )

        if h == 0:
            if part < 2:
                for k in range(2):
                    spot = group * 2 + k
                    one = send(part, region(part, at[far], spot, 1), w_line.at[part, spot], up)
                    if j == 0:
                        pl.when(spot != at[near])(one.wait_recv)
                    else:
                        one.wait_recv()
            elif j == 0:
                send(part, region(part, at[far], 0, 7), o_line.at[part - 2], up).wait_recv()
            leg(0, up).start()
            leg(0, down_).start()
        elif h < 3:
            leg(-h, up).wait_recv()
            leg(-h, up).start()
            leg(h, up).wait_recv()
            leg(h, down_).start()
        elif h == 3:
            leg(-3, up).wait_recv()
            if j < groups // 2:
                leg(-3, up).start()
            leg(3, up).wait_recv()
            if j >= groups // 2:
                leg(3, down_).start()
        else:
            leg(4, up).wait_recv()

    def ring(parts, h, js):
        for j in js:
            for part in parts:
                ring_step(part, h, j)

    def chunk(seq, q, device_id, own=False):
        return pltpu.make_async_remote_copy(
            src_ref=tokens.at[q] if own else T.at[seq, c, q], dst_ref=T.at[seq, c, q],
            send_sem=t_send, recv_sem=t_recv.at[seq, q], device_id=device_id, device_id_type=MESH,
        )

    def twin(seq, q, own=False):
        return pltpu.make_async_remote_copy(
            src_ref=tokens.at[q] if own else T.at[seq, c, q], dst_ref=T.at[seq, c, q],
            send_sem=p_send, recv_sem=p_recv.at[seq], device_id=partner, device_id_type=MESH,
        )

    def tokens_step(i):
        if i < 4:
            arrivals = ((left, i, right), (right, (i + 2) % 4, left))
        else:
            arrivals = ((across, i - 4, None), (across, i - 2, None))
        for seq, q, onward in arrivals:
            chunk(seq, q, partner).wait_recv()
            if i < 2:
                chunk(seq, q, {"fs": onward}).start()
            twin(seq, q).start()

    def twins(seq):
        pltpu.make_async_remote_copy(
            src_ref=T.at[seq, 1 - c], dst_ref=T.at[seq, 1 - c], send_sem=p_send,
            recv_sem=p_recv.at[seq], device_id=partner, device_id_type=MESH,
        ).wait_recv()

    phase("first_hops")
    first_hop(0)
    first_hop(1)
    for i in range(4):
        chunk(x, i, {"fs": right}, True).start()
        chunk(x, (i + 2) % 4, {"fs": left}, True).start()
    for q in range(4):
        twin(x, q, True).start()
    phase("ring0")
    ring((0, 1), 0, (0,))
    tokens_step(0)
    ring((0, 1), 0, (1, 2))
    tokens_step(1)
    ring((0, 1), 0, (3,))
    phase("ring1")
    ring((0, 1), 1, (0,))
    tokens_step(2)
    ring((0, 1), 1, (1, 2))
    tokens_step(3)
    ring((0, 1), 1, (3,))
    phase("ring2")
    twins(x)
    norm_rows(x, 1 - c)
    ring((0, 1), 2, (0,))
    norm_rows(left, c)
    ring((0, 1), 2, (1,))
    tokens_step(4)
    norm_rows(right, c)
    ring((0, 1), 2, (2,))
    twins(left)
    norm_rows(left, 1 - c)
    tokens_step(5)
    ring((0, 1), 2, (3,))
    phase("ring3")
    twins(right)
    norm_rows(right, 1 - c)
    ring((0, 1), 3, (0,))
    norm_rows(across, c)
    ring((0, 1), 3, (1,))
    twins(across)
    norm_rows(across, 1 - c)
    ring((0, 1), 3, (2, 3))
    first_hop(2)
    first_hop(3)

    phase("proj")
    lane = lax.broadcasted_iota(jnp.int32, (N, 16, 128), 2)

    def partial(spot):
        low = W[spot, :, 4]
        zero = jnp.zeros_like(low)
        low = jnp.stack([jnp.where(lane < 32, low, zero), jnp.where(lane >= 32, low, zero)], axis=1)
        maps = [W[spot, :, 0:2], W[spot, :, 2:4], low]
        maps = jnp.concatenate([m.reshape(256, 128) for m in maps], axis=1)
        return dot(normed[:, pl.ds(pl.multiple_of(spot * 256, 256), 256)], maps)

    acc[...] = partial(z)

    def add(i, carry):
        acc[...] += partial(wrap(z + i))
        return carry

    lax.fori_loop(1, 4, add, 0)
    lax.fori_loop(5, N, add, 0)
    phase("ring4")
    ring((0,), 4, range(4))
    phase("proj_last")
    proj = acc[...] + partial(wrap(z + 4))

    def tile(block):
        return W[:, :, block : block + 2].reshape(D, 128)

    low_rank = (proj[:, 256:288] + proj[:, 288:320]).astype(BF16)
    gate = dot(low_rank, pick(decay_up, 64, x, 4)) + pick(decay_bias, 64, x, 4)
    u = jnp.exp(-jnp.abs(gate))
    log1p = jnp.where(u < 0.01, u * (1.0 - u * (0.5 - u * (1.0 / 3.0))), jnp.log(1.0 + u))
    log_rate = (jnp.minimum(gate, 0.0) - log1p) / 16.0
    query = proj[:, 0:64].astype(BF16).astype(F32) * 64**-0.5
    key = proj[:, 64:128].astype(BF16).astype(F32)
    value = proj[:, 128:256].astype(BF16).astype(F32)

    phase("update")
    lower = lax.broadcasted_iota(jnp.int32, (64, 64), 0) >= lax.broadcasted_iota(jnp.int32, (64, 64), 1)
    ones = lower.astype(F32)
    spans = [slice(64 * i, 64 * (i + 1)) for i in range(2 * SEQS)]
    within = [dot(ones, log_rate[r], precision=HIGH) for r in spans]
    totals = [w[63:64] for w in within]
    column = [jnp.transpose(jnp.broadcast_to(t, (128, 64))) for t in totals]
    update = [
        dot(jnp.transpose(key[r] * jnp.exp(t - w)), value[r], precision=HIGH)
        for r, w, t in zip(spans, within, totals)
    ]
    for seq in range(SEQS):
        a, b = 2 * seq, 2 * seq + 1
        last = jnp.exp(column[b]) * update[a] + update[b]
        fall = column[a] + column[b]
        for half in range(2):
            part = slice(32 * half, 32 * (half + 1))
            state[a + half, 0] = last[part].astype(BF16)
            state[a + half, 1] = fall[part].astype(BF16)

    def spread(stage, name, src, dst):
        place = at[name]
        for d in (4, 3, 5, 2, 6, 1, 7):
            peer = wrap(place + d)
            pltpu.make_async_remote_copy(
                src_ref=src(peer), dst_ref=dst.at[place], send_sem=s_send.at[stage],
                recv_sem=s_recv.at[stage], device_id={name: peer}, device_id_type=MESH,
            ).start()

    def spread_all(stage, dst):
        ref = dst.at[0:7]
        return pltpu.make_async_remote_copy(
            src_ref=ref, dst_ref=ref, send_sem=s_send.at[stage], recv_sem=s_recv.at[stage],
            device_id=partner, device_id_type=MESH,
        )

    phase("spread0")
    spread(0, "sp_1", lambda i: state.at[i], got1)
    got1[y] = state[y]

    phase("ring4b")
    ring((1,), 4, range(4))
    phase("wproj")
    wproj = dot(normed[...], jnp.concatenate([tile(5), tile(7)], axis=1)).astype(BF16)
    for seq in range(SEQS):
        kv[seq] = wproj[128 * seq : 128 * (seq + 1), 128:256]
    wquery = wproj[:, 0:128] * 64**-0.5
    edge_copy = pltpu.make_async_remote_copy(
        src_ref=kv, dst_ref=edge, send_sem=e_sem.at[0], recv_sem=e_sem.at[1],
        device_id=after_id, device_id_type=MESH,
    )
    phase("out_ring0")
    ring((2, 3), 0, range(2))
    edge_copy.start()
    phase("local")
    q_dec = [query[r] * jnp.exp(w) for r, w in zip(spans, within)]
    scores = [
        dot(qd, key[r] * jnp.exp(-w), ((1,), (1,)), HIGH) for r, w, qd in zip(spans, within, q_dec)
    ]
    local = [
        dot(jnp.where(lower, s, 0.0), value[r], precision=HIGH) for r, s in zip(spans, scores)
    ]

    phase("wait0")
    spread_all(0, got1).wait_recv()
    phase("scan0")
    run = jnp.zeros((32, 128), F32)
    fall = jnp.zeros((32, 128), F32)
    prefix, falls = [], []
    for i in range(N):
        prefix.append(run)
        falls.append(fall)
        step = got1[i, 1].astype(F32)
        run = jnp.exp(step) * run + got1[i, 0].astype(F32)
        fall = fall + step
    tot[0] = run.astype(BF16)
    tot[1] = fall.astype(BF16)
    spread(1, "sp_0", lambda i: tot, got2)
    got2[z] = tot[...]

    phase("out_ring1")
    ring((2, 3), 1, range(2))
    phase("edge_wait")
    edge_copy.wait()
    phase("window")
    distance = (
        lax.broadcasted_iota(jnp.int32, (128, 256), 0)
        + 128
        - lax.broadcasted_iota(jnp.int32, (128, 256), 1)
    )
    first_key = jnp.where(me > 0, 0, 128)
    valid = (distance >= 0) & (distance < 128)
    valid = valid & (lax.broadcasted_iota(jnp.int32, (128, 256), 1) >= first_key)
    sinks = pick(sink, 2, x, 4)

    def window(seqs):
        bands = [jnp.concatenate([edge[seq], kv[seq]], axis=0) for seq in seqs for _ in range(2)]
        heads = [
            (wquery[128 * seq : 128 * (seq + 1), 64 * head : 64 * (head + 1)], sinks[:, head : head + 1])
            for seq in seqs
            for head in range(2)
        ]
        s = [dot(q, band[:, 0:64], ((1,), (1,))) for (q, _), band in zip(heads, bands)]
        s = [jnp.where(valid, a, -1e30) for a in s]
        top = [jnp.maximum(jnp.max(a, axis=-1, keepdims=True), h[1]) for a, h in zip(s, heads)]
        expo = [jnp.exp(a - t) for a, t in zip(s, top)]
        denom = [
            jnp.sum(e, axis=-1, keepdims=True) + jnp.exp(h[1] - t)
            for e, t, h in zip(expo, top, heads)
        ]
        weights = [(e * (1.0 / d)).astype(BF16) for e, d in zip(expo, denom)]
        got = [dot(w, band[:, 64:128]) for w, band in zip(weights, bands)]
        for i, seq in enumerate(seqs):
            hid[seq, :, 128:256] = jnp.concatenate(got[2 * i : 2 * i + 2], axis=1).astype(BF16)

    window((0, 1))
    phase("wait1")
    spread_all(1, got2).wait_recv()
    phase("scan1")
    come = jnp.zeros((32, 128), F32)
    for i in range(N):
        come = jnp.where(
            i < z, jnp.exp(got2[i, 1].astype(F32)) * come + got2[i, 0].astype(F32), come
        )
    for i in range(N):
        ret[i] = (jnp.exp(falls[i]) * come + prefix[i]).astype(BF16)
    spread(2, "sp_1", lambda i: ret.at[i], enter)
    enter[y] = ret[y]

    phase("out_ring2")
    ring((2, 3), 2, range(2))
    phase("window2")
    window((2, 3))
    phase("out_ring3")
    ring((2, 3), 3, range(2))
    phase("wait2")
    spread_all(2, enter).wait_recv()
    phase("gla_out")
    for seq in range(SEQS):
        a, b = 2 * seq, 2 * seq + 1
        come = jnp.concatenate([enter[a], enter[b]], axis=0).astype(F32)
        middle = jnp.exp(column[a]) * come + update[a]
        for i, entering in ((a, come), (b, middle)):
            gla = local[i] + dot(q_dec[i], entering, precision=HIGH)
            mean_square = jnp.mean(gla * gla, axis=-1, keepdims=True)
            gla = gla * lax.rsqrt(mean_square + EPS) * head_gain[...]
            hid[seq, 64 * (i - a) : 64 * (i - a + 1), 0:128] = gla.astype(BF16)
    phase("out_ring4")
    ring((2, 3), 4, range(2))

    phase("out_maps")
    out_map = jnp.concatenate([tile(9), tile(11)], axis=1)

    def to_partner(seq):
        return pltpu.make_async_remote_copy(
            src_ref=whole.at[seq, 1 - c], dst_ref=take.at[seq], send_sem=o_send,
            recv_sem=o_recv.at[seq], device_id=partner, device_id_type=MESH,
        )

    def multiply(seq):
        whole[seq] = dot(hid[seq], out_map, ((1,), (1,))).astype(BF16).reshape(2, 64, D)
        to_partner(seq).start()

    def chip_sum(seq):
        to_partner(seq).wait_recv()
        return whole[seq, c].astype(F32) + take[seq].astype(F32)

    def move(index, src, dst, device_id):
        return pltpu.make_async_remote_copy(
            src_ref=src, dst_ref=dst, send_sem=x_send, recv_sem=x_recv.at[index],
            device_id={"fs": device_id}, device_id_type=MESH,
        )

    moves = [
        move(0, hop.at[0], hopin.at[0], right), move(1, hop.at[1], hopin.at[1], left),
        move(2, fin.at[1], finin.at[1], right), move(3, fin.at[2], finin.at[2], left),
        move(4, fin.at[0], finin.at[0], right), move(5, fin.at[3], finin.at[3], left),
    ]
    multiply(across)
    multiply(right)
    phase("sum_across")
    s = chip_sum(across).astype(BF16)
    hop[0] = s[:, 0:1024]
    hop[1] = s[:, 1024:2048]
    moves[0].start()
    moves[1].start()
    phase("multiply_left")
    multiply(left)
    phase("sum_right")
    to_right = chip_sum(right)
    fin[1] = to_right[:, 1024:2048].astype(BF16)
    moves[2].start()
    phase("multiply_own")
    multiply(x)
    phase("sum_left")
    to_left = chip_sum(left)
    fin[2] = to_left[:, 0:1024].astype(BF16)
    moves[3].start()
    phase("hop_right")
    moves[0].wait_recv()
    fin[0] = (to_right[:, 0:1024] + hopin[0].astype(F32)).astype(BF16)
    moves[4].start()
    phase("hop_left")
    moves[1].wait_recv()
    fin[3] = (to_left[:, 1024:2048] + hopin[1].astype(F32)).astype(BF16)
    moves[5].start()
    phase("sum_own")
    mine = chip_sum(x)
    phase("last_wait")
    for i in (2, 3, 4, 5):
        moves[i].wait_recv()
    phase("write")
    low_half = mine[:, 0:1024] + finin[0].astype(F32) + finin[2].astype(F32)
    high_half = mine[:, 1024:2048] + finin[1].astype(F32) + finin[3].astype(F32)
    out[:, 0:1024] = low_half.astype(BF16)
    out[:, 1024:2048] = high_half.astype(BF16)

    phase("drain")

    def sent(ref, sem):
        pltpu.make_async_copy(ref, ref, sem).wait()

    for part in range(4):
        a, b, _, _ = PARTS[part]
        sent(W.at[0:7, :, a:b], w_send.at[part])
        sent(W.at[0, 0:7, a:b], w_send.at[part])
    sent(T.at[0:3, 0], t_send)
    sent(T.at[0:4, 0], p_send)
    for stage, ref in enumerate((got1, got2, enter)):
        spread_all(stage, ref).wait_send()
    sent(take, o_send)
    sent(take.at[0:3], x_send)
    scope.close()


def per_device(
    tokens, norm_gain, gla_query_weight, gla_key_weight, gla_value_weight, decay_down, decay_up,
    decay_bias, head_gain, window_query_weight, window_key_weight, window_value_weight, sink_logit,
    gla_output_weight, window_output_weight,
):
    operands = (
        tokens.reshape(4, 16, D),
        norm_gain.reshape(1, D),
        gla_query_weight,
        gla_key_weight,
        gla_value_weight,
        decay_down,
        decay_up,
        decay_bias.reshape(1, -1),
        head_gain.reshape(1, -1),
        window_query_weight,
        window_key_weight,
        window_value_weight,
        sink_logit.reshape(1, -1),
        gla_output_weight.T,
        window_output_weight.T,
    )
    dma, vmem = pltpu.SemaphoreType.DMA, pltpu.VMEM
    return pl.pallas_call(
        kernel,
        out_shape=jax.ShapeDtypeStruct((64, D), BF16),
        in_specs=[pl.BlockSpec(memory_space=pltpu.HBM)] * 15,
        out_specs=pl.BlockSpec(memory_space=pltpu.VMEM),
        scratch_shapes=[vmem(a.shape, a.dtype) for a in operands]
        + [
            dma((15,)),
            vmem((N, N, 13, 16, 128), BF16),
            vmem((4, 2, 4, 16, D), BF16),
            vmem((512, D), BF16),
            vmem((512, 384), F32),
            vmem((4, 128, 128), BF16),
            vmem((4, 128, 128), BF16),
            vmem((N, 2, 32, 128), BF16),
            vmem((N, 2, 32, 128), BF16),
            vmem((2, 32, 128), BF16),
            vmem((N, 2, 32, 128), BF16),
            vmem((N, 32, 128), BF16),
            vmem((N, 32, 128), BF16),
            vmem((4, 128, 256), BF16),
            vmem((4, 2, 64, D), BF16),
            vmem((4, 64, D), BF16),
            vmem((2, 64, 1024), BF16),
            vmem((2, 64, 1024), BF16),
            vmem((4, 64, 1024), BF16),
            vmem((4, 64, 1024), BF16),
            dma((4,)),
            dma((2, N)),
            dma((2, N, 4)),
            dma((2,)),
            dma((2, N, 2)),
            dma,
            dma((4, 4)),
            dma,
            dma((4,)),
            dma((2,)),
            dma((3,)),
            dma((3,)),
            dma,
            dma((4,)),
            dma,
            dma((6,)),
        ],
        compiler_params=pltpu.CompilerParams(
            collective_id=0, has_side_effects=True, vmem_limit_bytes=48 * 1024 * 1024
        ),
    )(*[pltpu.with_memory_space_constraint(a, pltpu.HBM) for a in operands])[None]


def solution(mesh):
    split = Mesh(
        mesh.devices.reshape(N, N, mesh.shape["fs"], mesh.shape["tp"]), ("sp_0", "sp_1", "fs", "tp")
    )
    return jax.shard_map(
        per_device,
        mesh=split,
        in_specs=(
            P("fs", SP_TP, None), P(), P(SP, "tp"), P(SP, "tp"), P(SP, "tp"), P(SP, None),
            P(None, "tp"), P("tp"), P(), P(SP, "tp"), P(SP, "tp"), P(SP, "tp"), P("tp"),
            P("tp", SP), P("tp", SP),
        ),
        out_specs=P("fs", SP_TP, None),
        check_vma=False,
    )
```

time: 88.1 us -> 73 us (0.83)
  local copies, waits for them, and re-layouts: 8.1 us -> 0.71 us
  Pallas kernels: 79.3 us -> 72.2 us
    unnamed x29 -> x1, local copies, waits for them, and re-layouts: 8.1 us -> 0.71 us
    pallas_call x1, Pallas kernels: 79.3 us -> 72.2 us  [per_device(): pl.pallas_call(kernel, out_shape=jax.ShapeDtypeStruct((64, D), BF16), in_...]
where the time goes in v3:
time: 73 us; the launch traced here: 72.9 us
  Pallas kernels  72.2 us (99%)
    pallas_call x1, Pallas kernels, per_device(): pl.pallas_call(kernel, out_shape=jax.ShapeDtypeStruct((64, D), BF16), in_...  72.2 us

profile of v3, /device:TPU:1, one launch (start us, length us, event | category | flops | bytes accessed | tf_op | source)
XLA Modules:
  0.0 72.9 jit_solution(15464660262296293240)
XLA Ops:
  0.0 72.2 %shard_map.145 = bf16[64,2048]{1,0:T(8,128)(2,1)S(1)} custom-call(bf16[4,16,2048]{2,1,0:T(8,128)(2,1)} %bitcast.9, f32[1,2048]{1,0:T(1,128)} %bitcast.12, bf16[32,256]{1,0:T(8,128)(2,1)} %refs_2_.1, bf16[32,256]{1,0:T(8,128)(2,1)} %refs_3_.1, bf16[32,512]{1,0:T(8,128)(2,1)} %refs_4_.1, bf16[32,32]{1,0:T(8,128)(2,1)} %refs_5_.1, bf16[32,256]{1,0:T(8,128)(2,1)} %refs_6_.1, ...), custom_call_target="tpu_custom_call" | custom-call | tf_op jit(solution)/shard_map/pallas_call | solution.py:552
  72.2 0.7 copy.17

commit v4 on v3

--- a/solution.py
+++ b/solution.py
@@ -10,20 +10,17 @@
 
 F32, BF16 = jnp.float32, jnp.bfloat16
 MESH = pl.DeviceIdType.MESH
-HIGH = lax.Precision.HIGHEST
 SP = ("sp_0", "sp_1")
 SP_TP = ("sp_0", "sp_1", "tp")
 EPS = 1e-06
 N = 8
 SEQS = 4
 D = 2048
-PARTS = ((0, 5, "sp_1", "sp_0"), (5, 9, "sp_0", "sp_1"), (9, 11, "sp_1", "sp_0"), (11, 13, "sp_0", "sp_1"))
-
-
-def dot(a, b, contract=((1,), (0,)), precision=None):
-    return lax.dot_general(
-        a, b, (contract, ((), ())), precision=precision, preferred_element_type=F32
-    )
+PARTS = ((0, 4, "sp_1", "sp_0"), (5, 9, "sp_0", "sp_1"), (9, 11, "sp_1", "sp_0"), (11, 13, "sp_0", "sp_1"))
+
+
+def dot(a, b, contract=((1,), (0,))):
+    return lax.dot_general(a, b, (contract, ((), ())), preferred_element_type=F32)
 
 
 def wrap(i, n=N):
@@ -33,9 +30,9 @@
 def kernel(*refs):
     sources, out, places = refs[:15], refs[15], refs[16:31]
     (
-        in_sems, W, T, normed, acc, kv, edge, state, got1, tot, got2, ret, enter, hid, whole, take,
+        in_sems, W, T, normed, acc, low_own, low_got, l_sem, kv, edge, state, got1, tot, got2, ret, enter, hid, whole, take,
         hop, hopin, fin, finin, w_send, w_line, w_far, o_line, o_far, t_send, t_recv, p_send,
-        p_recv, e_sem, s_send, s_recv, o_send, o_recv, x_send, x_recv,
+        p_recv, e_sem, s_send, s_recv, r_send, r_recv, o_send, o_recv, x_send, x_recv,
     ) = refs[31:]
     (
         tokens, norm_gain, gq, gk, gv, decay_down, decay_up, decay_bias, head_gain, wq, wk, wv,
@@ -48,6 +45,8 @@
         scope.enter_context(jax.named_scope(name))
 
     phase("greet")
+    for i in range(15):
+        pltpu.make_async_copy(sources[i], places[i], in_sems.at[i]).start()
     z, y = lax.axis_index("sp_0"), lax.axis_index("sp_1")
     x, c = lax.axis_index("fs"), lax.axis_index("tp")
     me = z * N + y
@@ -74,8 +73,6 @@
 
     phase("inputs")
     for i in range(15):
-        pltpu.make_async_copy(sources[i], places[i], in_sems.at[i]).start()
-    for i in range(15):
         pltpu.make_async_copy(sources[i], places[i], in_sems.at[i]).wait()
 
     phase("pack")
@@ -110,12 +107,12 @@
 
         lax.fori_loop(0, 4, body, 0)
 
-    norm_rows(x, c, tokens)
     phase("barrier")
     pl.semaphore_wait(barrier, 2 * (N - 1) + 5)
 
-    def region(part, far_spot, line_spot, count):
+    def region(part, far_spot, line_spot, count, longer=0):
         a, b, near, _ = PARTS[part]
+        b = b + longer
         line = pl.ds(line_spot, count)
         return W.at[far_spot, line, a:b] if near == "sp_1" else W.at[line, far_spot, a:b]
 
@@ -125,14 +122,28 @@
             device_id=device_id, device_id_type=MESH,
         )
 
-    def first_hop(part):
+    def each_core(part, act):
+        if part == 0:
+            pl.when(c == 0)(lambda: act(0))
+            pl.when(c == 1)(lambda: act(1))
+        else:
+            act(0)
+
+    def first_hop(part, by=(1, 7, 2, 6, 3, 5, 4)):
         _, _, near, far = PARTS[part]
-        ref = region(part, at[far], at[near], 1)
         sem = w_line.at[part, at[near]] if part < 2 else o_line.at[part - 2]
-        for d in (1, 7, 2, 6, 3, 5, 4):
-            send(part, ref, sem, {near: wrap(at[near] + d)}).start()
+
+        def act(longer):
+            ref = region(part, at[far], at[near], 1, longer)
+            for d in by:
+                send(part, ref, sem, {near: wrap(at[near] + d)}).start()
+
+        each_core(part, act)
 
     def ring_step(part, h, j):
+        each_core(part, lambda longer: ring_act(part, h, j, longer))
+
+    def ring_act(part, h, j, longer):
         _, _, near, far = PARTS[part]
         up, down_ = {far: wrap(at[far] + 1)}, {far: wrap(at[far] - 1)}
         if part < 2:
@@ -145,14 +156,17 @@
         def leg(far_by, device_id):
             spot = wrap(at[far] + far_by)
             return send(
-                part, region(part, spot, group * count, count), sems.at[spot, group], device_id
+                part, region(part, spot, group * count, count, longer), sems.at[spot, group],
+                device_id,
             )
 
         if h == 0:
             if part < 2:
                 for k in range(2):
                     spot = group * 2 + k
-                    one = send(part, region(part, at[far], spot, 1), w_line.at[part, spot], up)
+                    one = send(
+                        part, region(part, at[far], spot, 1, longer), w_line.at[part, spot], up
+                    )
                     if j == 0:
                         pl.when(spot != at[near])(one.wait_recv)
                     else:
@@ -218,6 +232,7 @@
         chunk(x, (i + 2) % 4, {"fs": left}, True).start()
     for q in range(4):
         twin(x, q, True).start()
+    norm_rows(x, c, tokens)
     phase("ring0")
     ring((0, 1), 0, (0,))
     tokens_step(0)
@@ -227,15 +242,23 @@
     phase("ring1")
     ring((0, 1), 1, (0,))
     tokens_step(2)
+    first_hop(2, (4,))
+    first_hop(3, (4,))
     ring((0, 1), 1, (1, 2))
     tokens_step(3)
+    first_hop(2, (3, 5))
+    first_hop(3, (3, 5))
     ring((0, 1), 1, (3,))
     phase("ring2")
     twins(x)
     norm_rows(x, 1 - c)
     ring((0, 1), 2, (0,))
+    first_hop(2, (2, 6))
+    first_hop(3, (2, 6))
     norm_rows(left, c)
     ring((0, 1), 2, (1,))
+    first_hop(2, (1, 7))
+    first_hop(3, (1, 7))
     tokens_step(4)
     norm_rows(right, c)
     ring((0, 1), 2, (2,))
@@ -251,11 +274,8 @@
     ring((0, 1), 3, (1,))
     twins(across)
     norm_rows(across, 1 - c)
-    ring((0, 1), 3, (2, 3))
-    first_hop(2)
-    first_hop(3)
-
-    phase("proj")
+    ring((0, 1), 3, (2,))
+
     lane = lax.broadcasted_iota(jnp.int32, (N, 16, 128), 2)
 
     def partial(spot):
@@ -267,6 +287,10 @@
         return dot(normed[:, pl.ds(pl.multiple_of(spot * 256, 256), 256)], maps)
 
     acc[...] = partial(z)
+    ring((0, 1), 3, (3,))
+    phase("out_ring0")
+    ring((2, 3), 0, range(2))
+    phase("proj")
 
     def add(i, carry):
         acc[...] += partial(wrap(z + i))
@@ -282,34 +306,52 @@
     def tile(block):
         return W[:, :, block : block + 2].reshape(D, 128)
 
-    low_rank = (proj[:, 256:288] + proj[:, 288:320]).astype(BF16)
+    lent = pltpu.make_async_remote_copy(
+        src_ref=low_own, dst_ref=low_got, send_sem=l_sem.at[0], recv_sem=l_sem.at[1],
+        device_id=partner, device_id_type=MESH,
+    )
+    low_rank = proj[:, 256:384]
+    low_rank = (low_rank + pltpu.roll(low_rank, 96, 1)).astype(BF16)
+    low_own[...] = low_rank
+    pl.when(c == 1)(lent.start)
+    pl.when(c == 0)(lent.wait_recv)
+    low_rank = jnp.where(c == 1, low_rank, low_got[...])[:, 0:32]
+    phase("out_ring1")
+    ring((2, 3), 1, range(2))
+    phase("gate")
     gate = dot(low_rank, pick(decay_up, 64, x, 4)) + pick(decay_bias, 64, x, 4)
     u = jnp.exp(-jnp.abs(gate))
     log1p = jnp.where(u < 0.01, u * (1.0 - u * (0.5 - u * (1.0 / 3.0))), jnp.log(1.0 + u))
     log_rate = (jnp.minimum(gate, 0.0) - log1p) / 16.0
     query = proj[:, 0:64].astype(BF16).astype(F32) * 64**-0.5
     key = proj[:, 64:128].astype(BF16).astype(F32)
-    value = proj[:, 128:256].astype(BF16).astype(F32)
+    value = proj[:, 128:256].astype(BF16)
 
     phase("update")
     lower = lax.broadcasted_iota(jnp.int32, (64, 64), 0) >= lax.broadcasted_iota(jnp.int32, (64, 64), 1)
-    ones = lower.astype(F32)
+    ones = jnp.concatenate([lower.astype(BF16)] * 3, axis=1)
+    high = log_rate.astype(BF16)
+    rest = log_rate - high.astype(F32)
+    middle = rest.astype(BF16)
+    rest = (rest - middle.astype(F32)).astype(BF16)
     spans = [slice(64 * i, 64 * (i + 1)) for i in range(2 * SEQS)]
-    within = [dot(ones, log_rate[r], precision=HIGH) for r in spans]
+    within = [dot(ones, jnp.concatenate([high[r], middle[r], rest[r]], axis=0)) for r in spans]
     totals = [w[63:64] for w in within]
     column = [jnp.transpose(jnp.broadcast_to(t, (128, 64))) for t in totals]
     update = [
-        dot(jnp.transpose(key[r] * jnp.exp(t - w)), value[r], precision=HIGH)
+        dot(jnp.transpose(key[r] * jnp.exp(t - w)).astype(BF16), value[r])
         for r, w, t in zip(spans, within, totals)
     ]
     for seq in range(SEQS):
         a, b = 2 * seq, 2 * seq + 1
         last = jnp.exp(column[b]) * update[a] + update[b]
-        fall = column[a] + column[b]
+        fall = jnp.concatenate([totals[a] + totals[b], jnp.zeros((1, 64), F32)], axis=1)
+        fall = jnp.broadcast_to(fall, (8, 128)).astype(BF16)
         for half in range(2):
-            part = slice(32 * half, 32 * (half + 1))
-            state[a + half, 0] = last[part].astype(BF16)
-            state[a + half, 1] = fall[part].astype(BF16)
+            for k in range(4):
+                at_row = 32 * half + 8 * k
+                state[a + half, k] = last[at_row : at_row + 8].astype(BF16)
+            state[a + half, 4] = fall
 
     def spread(stage, name, src, dst):
         place = at[name]
@@ -319,6 +361,19 @@
                 src_ref=src(peer), dst_ref=dst.at[place], send_sem=s_send.at[stage],
                 recv_sem=s_recv.at[stage], device_id={name: peer}, device_id_type=MESH,
             ).start()
+
+    def rows_total(peer, source):
+        return pltpu.make_async_remote_copy(
+            src_ref=tot, dst_ref=got2.at[source], send_sem=r_send.at[peer],
+            recv_sem=r_recv.at[source], device_id={"sp_0": peer}, device_id_type=MESH,
+        )
+
+    def slab(ref, i):
+        return jnp.concatenate([ref[i, k] for k in range(4)], axis=0).astype(F32)
+
+    def fall_of(row):
+        turned = jnp.transpose(jnp.broadcast_to(row[:, 0:64], (128, 64)))
+        return jnp.where(lax.rem(y, 2) == 0, turned[0:32], turned[32:64])
 
     def spread_all(stage, dst):
         ref = dst.at[0:7]
@@ -342,37 +397,54 @@
         src_ref=kv, dst_ref=edge, send_sem=e_sem.at[0], recv_sem=e_sem.at[1],
         device_id=after_id, device_id_type=MESH,
     )
-    phase("out_ring0")
-    ring((2, 3), 0, range(2))
+    phase("local")
+    q_dec = [(query[r] * jnp.exp(w)).astype(BF16) for r, w in zip(spans, within)]
+    scores = [
+        dot(qd, (key[r] * jnp.exp(-w)).astype(BF16), ((1,), (1,)))
+        for r, w, qd in zip(spans, within, q_dec)
+    ]
+    scores = [jnp.where(lower, s, 0.0).astype(BF16) for s in scores]
+    local = [dot(s, value[r]) for r, s in zip(spans, scores)]
     edge_copy.start()
-    phase("local")
-    q_dec = [query[r] * jnp.exp(w) for r, w in zip(spans, within)]
-    scores = [
-        dot(qd, key[r] * jnp.exp(-w), ((1,), (1,)), HIGH) for r, w, qd in zip(spans, within, q_dec)
-    ]
-    local = [
-        dot(jnp.where(lower, s, 0.0), value[r], precision=HIGH) for r, s in zip(spans, scores)
-    ]
-
+
+    phase("out_ring2")
+    ring((2, 3), 2, range(2))
     phase("wait0")
     spread_all(0, got1).wait_recv()
     phase("scan0")
+    rows = [got1[i, 4].astype(F32)[0:1] for i in range(N)]
+    steps = [fall_of(row) for row in rows]
     run = jnp.zeros((32, 128), F32)
     fall = jnp.zeros((32, 128), F32)
     prefix, falls = [], []
     for i in range(N):
         prefix.append(run)
         falls.append(fall)
-        step = got1[i, 1].astype(F32)
-        run = jnp.exp(step) * run + got1[i, 0].astype(F32)
-        fall = fall + step
-    tot[0] = run.astype(BF16)
-    tot[1] = fall.astype(BF16)
-    spread(1, "sp_0", lambda i: tot, got2)
-    got2[z] = tot[...]
-
-    phase("out_ring1")
-    ring((2, 3), 1, range(2))
+        run = jnp.exp(steps[i]) * run + slab(got1, i)
+        fall = fall + steps[i]
+    for k in range(4):
+        tot[k] = run[8 * k : 8 * (k + 1)].astype(BF16)
+    total_row = sum(rows[1:], rows[0])
+    tot[4] = jnp.broadcast_to(total_row, (8, 128)).astype(BF16)
+    for d in range(1, N):
+        peer = z + d
+        pl.when(peer < N)(rows_total(wrap(peer), z).start)
+
+    phase("out_ring3")
+    ring((2, 3), 3, range(2))
+    phase("wait1")
+    for i in range(N - 1):
+        pl.when(i < z)(rows_total(wrap(z + 1), i).wait_recv)
+    phase("scan1")
+    come = jnp.zeros((32, 128), F32)
+    for i in range(N - 1):
+        step = fall_of(got2[i, 4].astype(F32)[0:1])
+        come = jnp.where(i < z, jnp.exp(step) * come + slab(got2, i), come)
+    for i in range(N):
+        ret[i] = (jnp.exp(falls[i]) * come + prefix[i]).astype(BF16)
+    spread(2, "sp_1", lambda i: ret.at[i], enter)
+    enter[y] = ret[y]
+
     phase("edge_wait")
     edge_copy.wait()
     phase("window")
@@ -407,34 +479,17 @@
             hid[seq, :, 128:256] = jnp.concatenate(got[2 * i : 2 * i + 2], axis=1).astype(BF16)
 
     window((0, 1))
-    phase("wait1")
-    spread_all(1, got2).wait_recv()
-    phase("scan1")
-    come = jnp.zeros((32, 128), F32)
-    for i in range(N):
-        come = jnp.where(
-            i < z, jnp.exp(got2[i, 1].astype(F32)) * come + got2[i, 0].astype(F32), come
-        )
-    for i in range(N):
-        ret[i] = (jnp.exp(falls[i]) * come + prefix[i]).astype(BF16)
-    spread(2, "sp_1", lambda i: ret.at[i], enter)
-    enter[y] = ret[y]
-
-    phase("out_ring2")
-    ring((2, 3), 2, range(2))
     phase("window2")
     window((2, 3))
-    phase("out_ring3")
-    ring((2, 3), 3, range(2))
     phase("wait2")
     spread_all(2, enter).wait_recv()
     phase("gla_out")
     for seq in range(SEQS):
         a, b = 2 * seq, 2 * seq + 1
-        come = jnp.concatenate([enter[a], enter[b]], axis=0).astype(F32)
-        middle = jnp.exp(column[a]) * come + update[a]
+        come = jnp.concatenate([enter[a], enter[b]], axis=0)
+        middle = (jnp.exp(column[a]) * come.astype(F32) + update[a]).astype(BF16)
         for i, entering in ((a, come), (b, middle)):
-            gla = local[i] + dot(q_dec[i], entering, precision=HIGH)
+            gla = local[i] + dot(q_dec[i], entering)
             mean_square = jnp.mean(gla * gla, axis=-1, keepdims=True)
             gla = gla * lax.rsqrt(mean_square + EPS) * head_gain[...]
             hid[seq, 64 * (i - a) : 64 * (i - a + 1), 0:128] = gla.astype(BF16)
@@ -515,12 +570,19 @@
 
     for part in range(4):
         a, b, _, _ = PARTS[part]
-        sent(W.at[0:7, :, a:b], w_send.at[part])
-        sent(W.at[0, 0:7, a:b], w_send.at[part])
+
+        def gone(longer):
+            sent(W.at[0:7, :, a : b + longer], w_send.at[part])
+            sent(W.at[0, 0:7, a : b + longer], w_send.at[part])
+
+        each_core(part, gone)
+    pl.when(c == 1)(lent.wait_send)
     sent(T.at[0:3, 0], t_send)
     sent(T.at[0:4, 0], p_send)
-    for stage, ref in enumerate((got1, got2, enter)):
-        spread_all(stage, ref).wait_send()
+    spread_all(0, got1).wait_send()
+    spread_all(2, enter).wait_send()
+    for d in range(1, N):
+        pl.when(z + d < N)(rows_total(wrap(z + d), z).wait_send)
     sent(take, o_send)
     sent(take.at[0:3], x_send)
     scope.close()
@@ -561,12 +623,15 @@
             vmem((4, 2, 4, 16, D), BF16),
             vmem((512, D), BF16),
             vmem((512, 384), F32),
+            vmem((512, 128), BF16),
+            vmem((512, 128), BF16),
+            dma((2,)),
             vmem((4, 128, 128), BF16),
             vmem((4, 128, 128), BF16),
-            vmem((N, 2, 32, 128), BF16),
-            vmem((N, 2, 32, 128), BF16),
-            vmem((2, 32, 128), BF16),
-            vmem((N, 2, 32, 128), BF16),
+            vmem((N, 5, 8, 128), BF16),
+            vmem((N, 5, 8, 128), BF16),
+            vmem((5, 8, 128), BF16),
+            vmem((N, 5, 8, 128), BF16),
             vmem((N, 32, 128), BF16),
             vmem((N, 32, 128), BF16),
             vmem((4, 128, 256), BF16),
@@ -588,6 +653,8 @@
             dma((2,)),
             dma((3,)),
             dma((3,)),
+            dma((N,)),
+            dma((N,)),
             dma,
             dma((4,)),
             dma,

time: 73 us -> 68.2 us (0.934)
  Pallas kernels: 72.2 us -> 67.4 us
    pallas_call x1, Pallas kernels: 72.2 us -> 67.4 us  [per_device(): pl.pallas_call(kernel, out_shape=jax.ShapeDtypeStruct((64, D), BF16), in_...]
where the time goes in v4:
time: 68.2 us; the launch traced here: 68.1 us
  Pallas kernels  67.4 us (99%)
  local copies, waits for them, and re-layouts  0.71 us (1%)
    pallas_call x1, Pallas kernels, per_device(): pl.pallas_call(kernel, out_shape=jax.ShapeDtypeStruct((64, D), BF16), in_...  67.4 us

profile of v4, /device:TPU:1, one launch (start us, length us, event | category | flops | bytes accessed | tf_op | source)
XLA Modules:
  0.0 68.1 jit_solution(114218895462360627)
XLA Ops:
  0.0 67.4 %shard_map.145 = bf16[64,2048]{1,0:T(8,128)(2,1)S(1)} custom-call(bf16[4,16,2048]{2,1,0:T(8,128)(2,1)} %bitcast.9, f32[1,2048]{1,0:T(1,128)} %bitcast.12, bf16[32,256]{1,0:T(8,128)(2,1)} %refs_2_.1, bf16[32,256]{1,0:T(8,128)(2,1)} %refs_3_.1, bf16[32,512]{1,0:T(8,128)(2,1)} %refs_4_.1, bf16[32,32]{1,0:T(8,128)(2,1)} %refs_5_.1, bf16[32,256]{1,0:T(8,128)(2,1)} %refs_6_.1, ...), custom_call_target="tpu_custom_call" | custom-call | tf_op jit(solution)/shard_map/pallas_call | solution.py:614
  67.4 0.7 %copy.17 = bf16[1,64,2048]{2,1,0:T(8,128)(2,1)} copy(bf16[1,64,2048]{2,1,0:T(8,128)(2,1)S(1)} %bitcast.8) | data formatting | bytes 524288

commit v5 on v4

--- a/solution.py
+++ b/solution.py
@@ -10,6 +10,7 @@
 
 F32, BF16 = jnp.float32, jnp.bfloat16
 MESH = pl.DeviceIdType.MESH
+HIGH = lax.Precision.HIGHEST
 SP = ("sp_0", "sp_1")
 SP_TP = ("sp_0", "sp_1", "tp")
 EPS = 1e-06
@@ -19,8 +20,10 @@
 PARTS = ((0, 4, "sp_1", "sp_0"), (5, 9, "sp_0", "sp_1"), (9, 11, "sp_1", "sp_0"), (11, 13, "sp_0", "sp_1"))
 
 
-def dot(a, b, contract=((1,), (0,))):
-    return lax.dot_general(a, b, (contract, ((), ())), preferred_element_type=F32)
+def dot(a, b, contract=((1,), (0,)), precision=None):
+    return lax.dot_general(
+        a, b, (contract, ((), ())), precision=precision, preferred_element_type=F32
+    )
 
 
 def wrap(i, n=N):
@@ -95,17 +98,28 @@
     put(7, jnp.concatenate([pick(wk, 64, x // 2, 2), pick(wv, 64, x // 2, 2)], axis=1))
     put(9, pick(go, 128, x, 4))
     put(11, pick(wo, 128, x, 4))
-
-    def norm_rows(seq, half, source=None):
-        def body(q, carry):
-            rows = (T[seq, half, q] if source is None else source[q]).astype(F32)
-            mean_square = jnp.mean(rows * rows, axis=-1, keepdims=True)
-            rows = rows * lax.rsqrt(mean_square + EPS) * norm_gain[...]
-            index = (seq * 8 + half * 4 + q) * 16
-            normed[pl.ds(pl.multiple_of(index, 16), 16), :] = rows.astype(BF16)
+    for q in range(4):
+        T[x, c, q] = tokens[q]
+
+    def norm_rows():
+        def body(i, carry):
+            seq, half = i // 2, lax.rem(i, 2)
+            rows = pl.ds(pl.multiple_of(i * 64, 64), 64)
+            tiles = [slice(128 * k, 128 * (k + 1)) for k in range(D // 128)]
+
+            def load(k):
+                return T[seq, half, :, :, k].reshape(64, 128).astype(F32)
+
+            total = jnp.zeros((64, 128), F32)
+            for k in tiles:
+                total = total + load(k) * load(k)
+            mean_square = jnp.sum(total, axis=-1, keepdims=True) / D
+            factor = lax.rsqrt(mean_square + EPS)
+            for k in tiles:
+                normed[rows, k] = (load(k) * factor * norm_gain[:, k]).astype(BF16)
             return carry
 
-        lax.fori_loop(0, 4, body, 0)
+        lax.fori_loop(0, 2 * SEQS, body, 0)
 
     phase("barrier")
     pl.semaphore_wait(barrier, 2 * (N - 1) + 5)
@@ -131,7 +145,7 @@
 
     def first_hop(part, by=(1, 7, 2, 6, 3, 5, 4)):
         _, _, near, far = PARTS[part]
-        sem = w_line.at[part, at[near]] if part < 2 else o_line.at[part - 2]
+        sem = w_line.at[part, at[near] // 2] if part < 2 else o_line.at[part - 2]
 
         def act(longer):
             ref = region(part, at[far], at[near], 1, longer)
@@ -162,15 +176,8 @@
 
         if h == 0:
             if part < 2:
-                for k in range(2):
-                    spot = group * 2 + k
-                    one = send(
-                        part, region(part, at[far], spot, 1, longer), w_line.at[part, spot], up
-                    )
-                    if j == 0:
-                        pl.when(spot != at[near])(one.wait_recv)
-                    else:
-                        one.wait_recv()
+                ref = region(part, at[far], group * 2, 1 if j == 0 else 2, longer)
+                send(part, ref, w_line.at[part, group], up).wait_recv()
             elif j == 0:
                 send(part, region(part, at[far], 0, 7), o_line.at[part - 2], up).wait_recv()
             leg(0, up).start()
@@ -178,15 +185,15 @@
         elif h < 3:
             leg(-h, up).wait_recv()
             leg(-h, up).start()
+            if h == 2 and j < groups // 2:
+                leg(-2, {far: wrap(at[far] + 2)}).start()
             leg(h, up).wait_recv()
             leg(h, down_).start()
+            if h == 2 and j >= groups // 2:
+                leg(2, {far: wrap(at[far] - 2)}).start()
         elif h == 3:
             leg(-3, up).wait_recv()
-            if j < groups // 2:
-                leg(-3, up).start()
             leg(3, up).wait_recv()
-            if j >= groups // 2:
-                leg(3, down_).start()
         else:
             leg(4, up).wait_recv()
 
@@ -232,7 +239,6 @@
         chunk(x, (i + 2) % 4, {"fs": left}, True).start()
     for q in range(4):
         twin(x, q, True).start()
-    norm_rows(x, c, tokens)
     phase("ring0")
     ring((0, 1), 0, (0,))
     tokens_step(0)
@@ -251,30 +257,19 @@
     ring((0, 1), 1, (3,))
     phase("ring2")
     twins(x)
-    norm_rows(x, 1 - c)
     ring((0, 1), 2, (0,))
     first_hop(2, (2, 6))
     first_hop(3, (2, 6))
-    norm_rows(left, c)
     ring((0, 1), 2, (1,))
     first_hop(2, (1, 7))
     first_hop(3, (1, 7))
     tokens_step(4)
-    norm_rows(right, c)
     ring((0, 1), 2, (2,))
     twins(left)
-    norm_rows(left, 1 - c)
     tokens_step(5)
     ring((0, 1), 2, (3,))
-    phase("ring3")
     twins(right)
-    norm_rows(right, 1 - c)
-    ring((0, 1), 3, (0,))
-    norm_rows(across, c)
-    ring((0, 1), 3, (1,))
     twins(across)
-    norm_rows(across, 1 - c)
-    ring((0, 1), 3, (2,))
 
     lane = lax.broadcasted_iota(jnp.int32, (N, 16, 128), 2)
 
@@ -286,18 +281,24 @@
         maps = jnp.concatenate([m.reshape(256, 128) for m in maps], axis=1)
         return dot(normed[:, pl.ds(pl.multiple_of(spot * 256, 256), 256)], maps)
 
+    phase("norm")
+    norm_rows()
+    phase("proj")
     acc[...] = partial(z)
-    ring((0, 1), 3, (3,))
-    phase("out_ring0")
-    ring((2, 3), 0, range(2))
-    phase("proj")
 
     def add(i, carry):
         acc[...] += partial(wrap(z + i))
         return carry
 
-    lax.fori_loop(1, 4, add, 0)
-    lax.fori_loop(5, N, add, 0)
+    lax.fori_loop(1, 3, add, 0)
+    lax.fori_loop(6, N, add, 0)
+    phase("out_ring0")
+    ring((2, 3), 0, range(2))
+    phase("ring3")
+    ring((0,), 3, range(4))
+    phase("proj3")
+    add(3, 0)
+    add(5, 0)
     phase("ring4")
     ring((0,), 4, range(4))
     phase("proj_last")
@@ -316,8 +317,6 @@
     pl.when(c == 1)(lent.start)
     pl.when(c == 0)(lent.wait_recv)
     low_rank = jnp.where(c == 1, low_rank, low_got[...])[:, 0:32]
-    phase("out_ring1")
-    ring((2, 3), 1, range(2))
     phase("gate")
     gate = dot(low_rank, pick(decay_up, 64, x, 4)) + pick(decay_bias, 64, x, 4)
     u = jnp.exp(-jnp.abs(gate))
@@ -386,7 +385,10 @@
     spread(0, "sp_1", lambda i: state.at[i], got1)
     got1[y] = state[y]
 
+    phase("out_ring1")
+    ring((2, 3), 1, range(2))
     phase("ring4b")
+    ring((1,), 3, range(4))
     ring((1,), 4, range(4))
     phase("wproj")
     wproj = dot(normed[...], jnp.concatenate([tile(5), tile(7)], axis=1)).astype(BF16)
@@ -397,15 +399,16 @@
         src_ref=kv, dst_ref=edge, send_sem=e_sem.at[0], recv_sem=e_sem.at[1],
         device_id=after_id, device_id_type=MESH,
     )
+    edge_copy.start()
     phase("local")
-    q_dec = [(query[r] * jnp.exp(w)).astype(BF16) for r, w in zip(spans, within)]
+    q_dec = [query[r] * jnp.exp(w) for r, w in zip(spans, within)]
     scores = [
-        dot(qd, (key[r] * jnp.exp(-w)).astype(BF16), ((1,), (1,)))
+        dot(qd, key[r] * jnp.exp(-w), ((1,), (1,)), HIGH)
         for r, w, qd in zip(spans, within, q_dec)
     ]
-    scores = [jnp.where(lower, s, 0.0).astype(BF16) for s in scores]
-    local = [dot(s, value[r]) for r, s in zip(spans, scores)]
-    edge_copy.start()
+    scores = [jnp.where(lower, s, 0.0) for s in scores]
+    local = [dot(s, value[r].astype(F32), precision=HIGH) for r, s in zip(spans, scores)]
+    q_dec = [qd.astype(BF16) for qd in q_dec]
 
     phase("out_ring2")
     ring((2, 3), 2, range(2))
@@ -430,8 +433,6 @@
         peer = z + d
         pl.when(peer < N)(rows_total(wrap(peer), z).start)
 
-    phase("out_ring3")
-    ring((2, 3), 3, range(2))
     phase("wait1")
     for i in range(N - 1):
         pl.when(i < z)(rows_total(wrap(z + 1), i).wait_recv)
@@ -494,6 +495,7 @@
             gla = gla * lax.rsqrt(mean_square + EPS) * head_gain[...]
             hid[seq, 64 * (i - a) : 64 * (i - a + 1), 0:128] = gla.astype(BF16)
     phase("out_ring4")
+    ring((2, 3), 3, range(2))
     ring((2, 3), 4, range(2))
 
     phase("out_maps")
@@ -642,7 +644,7 @@
             vmem((4, 64, 1024), BF16),
             vmem((4, 64, 1024), BF16),
             dma((4,)),
-            dma((2, N)),
+            dma((2, 4)),
             dma((2, N, 4)),
             dma((2,)),
             dma((2, N, 2)),

time: 68.2 us -> 66.6 us (0.977)
  Pallas kernels: 67.4 us -> 65.7 us
    pallas_call x1, Pallas kernels: 67.4 us -> 65.7 us  [per_device(): pl.pallas_call(kernel, out_shape=jax.ShapeDtypeStruct((64, D), BF16), in_...]
where the time goes in v5:
time: 66.6 us; the launch traced here: 66.4 us
  Pallas kernels  65.7 us (99%)
  local copies, waits for them, and re-layouts  0.71 us (1%)
    pallas_call x1, Pallas kernels, per_device(): pl.pallas_call(kernel, out_shape=jax.ShapeDtypeStruct((64, D), BF16), in_...  65.7 us

profile of v5, /device:TPU:1, one launch (start us, length us, event | category | flops | bytes accessed | tf_op | source)
XLA Modules:
  0.0 66.4 jit_solution(6325469141130175252)
XLA Ops:
  0.0 65.7 %shard_map.145 = bf16[64,2048]{1,0:T(8,128)(2,1)S(1)} custom-call(bf16[4,16,2048]{2,1,0:T(8,128)(2,1)} %bitcast.9, f32[1,2048]{1,0:T(1,128)} %bitcast.12, bf16[32,256]{1,0:T(8,128)(2,1)} %refs_2_.1, bf16[32,256]{1,0:T(8,128)(2,1)} %refs_3_.1, bf16[32,512]{1,0:T(8,128)(2,1)} %refs_4_.1, bf16[32,32]{1,0:T(8,128)(2,1)} %refs_5_.1, bf16[32,256]{1,0:T(8,128)(2,1)} %refs_6_.1, ...), custom_call_target="tpu_custom_call" | custom-call | tf_op jit(solution)/shard_map/pallas_call | solution.py:616
  65.7 0.7 %copy.17 = bf16[1,64,2048]{2,1,0:T(8,128)(2,1)} copy(bf16[1,64,2048]{2,1,0:T(8,128)(2,1)S(1)} %bitcast.8) | data formatting | bytes 524288

commit v6 on v5

--- a/solution.py
+++ b/solution.py
@@ -240,21 +240,19 @@
     for q in range(4):
         twin(x, q, True).start()
     phase("ring0")
-    ring((0, 1), 0, (0,))
+    ring((0, 1), 0, range(4))
     tokens_step(0)
-    ring((0, 1), 0, (1, 2))
     tokens_step(1)
-    ring((0, 1), 0, (3,))
     phase("ring1")
     ring((0, 1), 1, (0,))
     tokens_step(2)
     first_hop(2, (4,))
     first_hop(3, (4,))
     ring((0, 1), 1, (1, 2))
-    tokens_step(3)
     first_hop(2, (3, 5))
     first_hop(3, (3, 5))
     ring((0, 1), 1, (3,))
+    tokens_step(3)
     phase("ring2")
     twins(x)
     ring((0, 1), 2, (0,))
@@ -264,10 +262,9 @@
     first_hop(2, (1, 7))
     first_hop(3, (1, 7))
     tokens_step(4)
-    ring((0, 1), 2, (2,))
+    ring((0, 1), 2, (2, 3))
+    tokens_step(5)
     twins(left)
-    tokens_step(5)
-    ring((0, 1), 2, (3,))
     twins(right)
     twins(across)
 

time: 66.6 us -> 66.5 us (level)
  no operation moved by 1% of the time
where the time goes in v6:
time: 66.5 us; the launch traced here: 66.4 us
  Pallas kernels  65.7 us (99%)
  local copies, waits for them, and re-layouts  0.71 us (1%)
    pallas_call x1, Pallas kernels, per_device(): pl.pallas_call(kernel, out_shape=jax.ShapeDtypeStruct((64, D), BF16), in_...  65.7 us

profile of v6, /device:TPU:1, one launch (start us, length us, event | category | flops | bytes accessed | tf_op | source)
XLA Modules:
  0.0 66.4 jit_solution(12800086677231211513)
XLA Ops:
  0.0 65.7 %shard_map.145 = bf16[64,2048]{1,0:T(8,128)(2,1)S(1)} custom-call(bf16[4,16,2048]{2,1,0:T(8,128)(2,1)} %bitcast.9, f32[1,2048]{1,0:T(1,128)} %bitcast.12, bf16[32,256]{1,0:T(8,128)(2,1)} %refs_2_.1, bf16[32,256]{1,0:T(8,128)(2,1)} %refs_3_.1, bf16[32,512]{1,0:T(8,128)(2,1)} %refs_4_.1, bf16[32,32]{1,0:T(8,128)(2,1)} %refs_5_.1, bf16[32,256]{1,0:T(8,128)(2,1)} %refs_6_.1, ...), custom_call_target="tpu_custom_call" | custom-call | tf_op jit(solution)/shard_map/pallas_call | solution.py:613
  65.7 0.7 %copy.17 = bf16[1,64,2048]{2,1,0:T(8,128)(2,1)} copy(bf16[1,64,2048]{2,1,0:T(8,128)(2,1)S(1)} %bitcast.8) | data formatting | bytes 524288
